TPU v7x, 256 devices: a whole 4x4x8 slice. The times are simulated.
256 devices in a mesh: rep: 2 (over z_hi), fs: 16 (over z_lo, y), tp: 8 (over x, core).
Axes of the slice: x: 4, y: 4, z: 8 (z_hi: 2, z_lo: 4; z = z_hi * 4 + z_lo), core: 2. Of those that a mesh axis runs over, the one named last changes fastest.
Arguments:
- tokens: bfloat16 [49152, 2048], P(('rep', 'fs', 'tp')), may hold values from -6 to 6
- mix_gain_in: float32 [2048], replicated, may hold values from 0.1 to 1.9
- pool_weight: bfloat16 [4, 512, 512], P(None, 'fs'), may hold values from -0.25 to 0.25
- mix_gain_out: float32 [2048], replicated, may hold values from 0.1 to 1.9
- ffn_gain_in: float32 [2048], replicated, may hold values from 0.1 to 1.9
- gate_weight: bfloat16 [2048, 5632], P('fs', 'tp'), may hold values from -0.125 to 0.125
- up_weight: bfloat16 [2048, 5632], P('fs', 'tp'), may hold values from -0.125 to 0.125
- gate_taps: float32 [3, 5632], replicated, may hold values from -3.5 to 3.5
- up_taps: float32 [3, 5632], replicated, may hold values from -3.5 to 3.5
- down_weight: bfloat16 [5632, 2048], P('tp', 'fs'), may hold values from -0.078125 to 0.078125
- ffn_gain_out: float32 [2048], replicated, may hold values from 0.1 to 1.9
Outputs:
- mixed_out: bfloat16 [49152, 2048], P(('rep', 'fs', 'tp'))
All inputs are finite; a program needn't handle non-finite values.
Results may differ from a plain program's by a relative error of at most 0.014.
Values may be sent and summed in bfloat16 or wider, within the bound.
A program may use at most 128 MiB of HBM per device.

v0:
```python
import jax
import jax.numpy as jnp
from jax import lax
from jax.sharding import PartitionSpec as P

pool_spans = (2, 4, 8, 16)
rms_eps = 1e-06


def sent_to_all(x, axis):
    copies = jnp.broadcast_to(x, (lax.axis_size(axis), *x.shape))
    return lax.all_to_all(copies, axis, split_axis=0, concat_axis=0, tiled=True)


def joined_along(tiles, dim):
    dims = list(tiles.shape[1:])
    dims[dim] *= tiles.shape[0]
    return jnp.moveaxis(tiles, 0, dim).reshape(dims)


def gathered_copies(x, axis, dim):
    tiles = sent_to_all(x, axis)
    return joined_along(tiles, dim)


def sent_together(arrays, axis, dim, along):
    ends, at = ([], 0)
    for a in arrays[:-1]:
        at += a.shape[along]
        ends.append(at)
    both = jnp.concatenate(arrays, axis=along)
    return tuple(jnp.split(lax.all_gather(both, axis, axis=dim, tiled=True), ends, axis=along))


def rms_scale(values, gain):
    floats = values.astype(jnp.float32)
    return floats * lax.rsqrt(jnp.mean(floats * floats, axis=-1, keepdims=True) + rms_eps) * gain


def pooled_gap(padded, count):
    margin = padded.shape[0] - count
    floats = padded.astype(jnp.float32)
    width = padded.shape[1] // len(pool_spans)
    where = jnp.arange(count, dtype=jnp.int32)
    pieces = []
    for group, span in enumerate(pool_spans):
        block = floats[:, group * width : (group + 1) * width]
        total = jnp.zeros((count, width), jnp.float32)
        for back in range(span):
            total = total + block[margin - back : margin - back + count]
        divisor = jnp.minimum(where + 1, span).astype(jnp.float32)
        pieces.append(total / divisor[:, None] - block[margin:])
    return jnp.concatenate(pieces, axis=1).astype(jnp.bfloat16)


def mix_groups(gap, pool_full):
    length, features = gap.shape
    groups = pool_full.shape[0]
    shaped = gap.reshape(length, groups, features // groups)
    result = jnp.einsum("rgc,gcj->rgj", shaped, pool_full, preferred_element_type=jnp.float32)
    return result.reshape(length, features).astype(jnp.bfloat16)


def causal_taps(pre, taps):
    width = taps.shape[0]
    floats = pre.astype(jnp.float32)
    padded = jnp.concatenate([jnp.zeros((width - 1, pre.shape[1]), jnp.float32), floats], axis=0)
    total = jnp.zeros(floats.shape, jnp.float32)
    for offset in range(width):
        total = total + taps[offset] * padded[offset : offset + pre.shape[0]]
    return total


def shards(
    tokens,
    mix_gain_in,
    pool_weight,
    mix_gain_out,
    ffn_gain_in,
    gate_weight,
    up_weight,
    gate_taps,
    up_taps,
    down_weight,
    ffn_gain_out,
):
    rows, features = tokens.shape
    margin = max(pool_spans) - 1
    position = lax.axis_index("tp")
    pool_full = gathered_copies(pool_weight, "fs", 1)
    every = lax.all_gather(tokens, "tp", axis=0, tiled=True)
    length = every.shape[0]
    normed = rms_scale(every, mix_gain_in).astype(jnp.bfloat16)
    padded = jnp.concatenate([jnp.zeros((margin, features), jnp.bfloat16), normed], axis=0)
    gap = pooled_gap(padded, length)
    mixed = mix_groups(gap, pool_full)
    after_all = every.astype(jnp.float32) + rms_scale(mixed, mix_gain_out)
    whole = rms_scale(after_all, ffn_gain_in).astype(jnp.bfloat16)
    after_mix = lax.dynamic_slice_in_dim(after_all, position * rows, rows, 0)
    columns = gate_weight.shape[1]
    pieces = sent_together((gate_weight, up_weight), "fs", 0, 1)
    gate_part = jnp.dot(whole, pieces[0], preferred_element_type=jnp.float32)
    up_part = jnp.dot(whole, pieces[1], preferred_element_type=jnp.float32)
    offset = position * columns
    gate_local = lax.dynamic_slice_in_dim(gate_taps, offset, columns, 1)
    up_local = lax.dynamic_slice_in_dim(up_taps, offset, columns, 1)
    gate_conv = causal_taps(gate_part.astype(jnp.bfloat16), gate_local)
    up_conv = causal_taps(up_part.astype(jnp.bfloat16), up_local)
    hidden = (jax.nn.gelu(gate_conv, approximate=True) * up_conv).astype(jnp.bfloat16)
    down_full = gathered_copies(down_weight, "fs", 1)
    channel_out = lax.psum_scatter(
        jnp.dot(hidden, down_full, preferred_element_type=jnp.float32).astype(jnp.bfloat16),
        "tp",
        scatter_dimension=0,
        tiled=True,
    ).astype(jnp.float32)
    return (after_mix + rms_scale(channel_out, ffn_gain_out)).astype(jnp.bfloat16)


def solution(mesh):
    in_specs = (
        P(("rep", "fs", "tp"), None),
        P(),
        P(None, "fs", None),
        P(),
        P(),
        P("fs", "tp"),
        P("fs", "tp"),
        P(),
        P(),
        P("tp", "fs"),
        P(),
    )
    out_specs = P(("rep", "fs", "tp"), None)
    return jax.shard_map(shards, mesh=mesh, in_specs=in_specs, out_specs=out_specs, check_vma=False)
```

profile of v0, /device:TPU:1, one launch (start us, length us, event | category | flops | bytes accessed | tf_op | source)
XLA Modules:
  0.0 308.5 jit_solution(7693854156500946584)
XLA Ops:
  6.5 0.0 all-gather.3.cloned.1.call-start
  6.5 0.7 all-gather.3.cloned.1.call-update
  7.3 0.0 copy-start.3
  7.3 0.0 copy-start.4
  7.3 2.6 broadcast_in_dim.4
  9.8 0.0 copy-start.5
  9.8 9.3 %all-to-all-start = ((bf16[16,4,32,512]{3,2,1,0:T(8,128)(2,1)}), bf16[16,4,32,512]{3,2,1,0:T(8,128)(2,1)S(1)}, u32[]{:S(2)}, u32[]{:S(2)}) async-start(bf16[16,4,32,512]{3,2,1,0:T(8,128)(2,1)} %broadcast_in_dim.4), calls=%async_computation | async-start | bytes 4194304 | tf_op jit(solution)/shard_map/all_to_all | solution.py:12
  19.1 0.0 all-gather.5.cloned.1.call-start
  19.2 0.0 copy-done.3
  19.2 0.0 copy-done.4
  19.2 0.8 pad_maximum_fusion
  20.0 0.0 all-gather.5.cloned.1.call-update
  20.0 1.0 dynamic-slice_reduce_fusion.2
  21.0 39.6 %all-to-all-done = bf16[16,4,32,512]{3,2,1,0:T(8,128)(2,1)S(1)} async-done(((bf16[16,4,32,512]{3,2,1,0:T(8,128)(2,1)}), bf16[16,4,32,512]{3,2,1,0:T(8,128)(2,1)S(1)}, u32[]{:S(2)}, u32[]{:S(2)}) %all-to-all-start) | async-done | bytes 2097184 | tf_op jit(solution)/shard_map/all_to_all | solution.py:12
  60.7 0.0 copy-done.5
  60.7 2.1 broadcast_in_dim.5
  62.8 11.0 %all-to-all-start.1 = ((bf16[16,704,128]{2,1,0:T(8,128)(2,1)}), bf16[16,704,128]{2,1,0:T(8,128)(2,1)}, u32[]{:S(2)}, u32[]{:S(2)}) async-start(bf16[16,704,128]{2,1,0:T(8,128)(2,1)} %broadcast_in_dim.5), calls=%async_computation.1 | async-start | bytes 5767168 | tf_op jit(solution)/shard_map/all_to_all | solution.py:12
  73.9 0.0 reduce-scatter.2.cloned.1.call-start
  73.9 1.5 copy.16
  75.4 0.0 copy-start.6
  75.4 0.0 all-gather.3.cloned.1.call-done
  75.4 4.2 %fusion = f32[1536]{0:T(1024)S(1)} fusion(bf16[1536,2048]{1,0:T(8,128)(2,1)} %all-gather.3.cloned.1.call-done), kind=kLoop, calls=%fused_computation.3 | loop fusion | flops 9435648 | bytes 6297600 | tf_op jit(solution)/shard_map/reduce_sum | solution.py:37
  79.6 0.0 copy-done.6
  79.7 0.4 copy-done
  80.0 4.2 %fusion.2 = bf16[1536,2048]{1,0:T(8,128)(2,1)} fusion(bf16[1536,2048]{1,0:T(8,128)(2,1)S(1)} %copy-done, f32[2048]{0:T(1024)S(1)} %copy-done.6, f32[1536]{0:T(1024)S(1)} %add_rsqrt_fusion.2), kind=kLoop, calls=%fused_computation.5 | loop fusion | flops 12582912 | bytes 12597248 | tf_op jit(solution)/shard_map/convert_element_type | solution.py:93
  84.2 4.6 %pad_convert_fusion = f32[1551,2048]{1,0:T(8,128)S(1)} fusion(bf16[1536,2048]{1,0:T(8,128)(2,1)} %fusion.2), kind=kLoop, calls=%fused_computation.11 | loop fusion | flops 3176448 | bytes 18997248 | tf_op jit(solution)/shard_map/convert_element_type | solution.py:42
  88.8 5.2 %fusion.53 = (bf16[1536,1,512]{2,0,1:T(8,128)(2,1)S(1)}, bf16[1536,1,512]{2,0,1:T(8,128)(2,1)S(1)}, bf16[1536,1,512]{2,0,1:T(8,128)(2,1)S(1)}) fusion(f32[1536]{0:T(1024)S(1)} %minimum_convert_fusion.3, f32[1551,2048]{1,0:T(8,128)S(1)} %pad_convert_fusion, f32[1536]{0:T(1024)S(1)} %get-tuple-element.19, f32[1536]{0:T(1024)S(1)} %get-tuple-element.18), kind=kLoop, calls=%fused_computation.94 | loop fusion | flops 15728640 | bytes 48777216 | tf_op jit(solution)/shard_map/concatenate | solution.py:53
  94.0 0.0 copy-start.2
  94.0 6.2 %fusion.56 = bf16[1536,1,512]{2,0,1:T(8,128)(2,1)} fusion(f32[1536]{0:T(1024)S(1)} %minimum_convert_fusion, f32[1551,2048]{1,0:T(8,128)S(1)} %pad_convert_fusion), kind=kLoop, calls=%fused_computation.97 | loop fusion | flops 14155776 | bytes 51910656 | tf_op jit(solution)/shard_map/concatenate | solution.py:53
  100.2 0.0 copy-done.2
  100.2 7.7 %multiply_reduce_fusion.1 = (f32[1536]{0:T(1024)S(1)}, f32[4,1536,512]{1,2,0:T(8,128)}) fusion(bf16[4,512,512]{2,1,0:T(8,128)(2,1)S(1)} %bitcast.24, bf16[1536,1,512]{2,0,1:T(8,128)(2,1)} %fusion.56, bf16[1536,1,512]{2,0,1:T(8,128)(2,1)S(1)} %get-tuple-element.15, bf16[1536,1,512]{2,0,1:T(8,128)(2,1)S(1)} %get-tuple-element.14, ...), kind=kOutput, calls=%fused_computation.8 | convolution fusion | flops 3243244032 | bytes 20977664 | tf_op jit(solution)/shard_map/rgc,gcj->rgj/dot_general | solution.py:60
  107.9 12.6 %copy.21 = f32[1536,2048]{1,0:T(8,128)} copy(f32[1536,2048]{0,1:T(8,128)} %bitcast.23) | data formatting | bytes 25165824 | tf_op jit(solution)/shard_map/convert_element_type | solution.py:36
  120.5 0.0 copy-done.8
  120.5 0.0 copy-start.10
  120.5 12.7 %multiply_reduce_fusion = (f32[1536]{0:T(1024)S(1)}, f32[1536,2048]{1,0:T(8,128)}) fusion(f32[2048]{0:T(1024)S(1)} %copy-done.8, f32[1536,2048]{1,0:T(8,128)} %copy.21, f32[1536]{0:T(1024)S(1)} %add_rsqrt_fusion.1, bf16[1536,2048]{1,0:T(8,128)(2,1)} %all-gather.3.cloned.1.call-done), kind=kLoop, calls=%fused_computation.7 | loop fusion | flops 18872832 | bytes 31477760 | tf_op jit(solution)/shard_map/reduce_sum | solution.py:37
  133.3 68.4 %all-gather.5.cloned.1.call-done = bf16[2048,1408]{0,1:T(8,128)(2,1)} async-done(((bf16[128,1408]{0,1:T(8,128)(2,1)}), bf16[2048,1408]{0,1:T(8,128)(2,1)}) %all-gather.5.cloned.1.call-update) | async-done | bytes 5767184 | tf_op jit(solution)/shard_map/all_gather | solution.py:32
  201.6 0.0 copy-done.10
  201.7 12.3 %fusion.31 = f32[1536,704]{0,1:T(8,128)} fusion(bf16[2048,1408]{0,1:T(8,128)(2,1)} %all-gather.5.cloned.1.call-done, f32[1536,2048]{1,0:T(8,128)} %get-tuple-element.12, f32[2048]{0:T(1024)S(1)} %copy-done.10, f32[1536]{0:T(1024)S(1)} %add_rsqrt_fusion), kind=kOutput, calls=%fused_computation.45 | convolution fusion | flops 4440784896 | bytes 19806208 | tf_op jit(solution)/shard_map/dot_general | solution.py:102
  214.0 0.0 copy-done.1
  214.0 0.0 copy-done.9
  214.0 6.7 %fusion.30 = f32[1536,704]{0,1:T(8,128)} fusion(bf16[2048,1408]{0,1:T(8,128)(2,1)S(1)} %copy-done.9, f32[1536,2048]{1,0:T(8,128)S(1)} %copy-done.1, f32[2048]{0:T(1024)S(1)} %copy-done.10, f32[1536]{0:T(1024)S(1)} %add_rsqrt_fusion), kind=kOutput, calls=%fused_computation.43 | convolution fusion | flops 4440784896 | bytes 19808256 | tf_op jit(solution)/shard_map/dot_general | solution.py:103
  220.7 0.0 all-to-all-done.1
  220.7 21.6 %convolution_convert_fusion = bf16[1536,2048]{1,0:T(8,128)(2,1)} fusion(f32[1536,704]{0,1:T(8,128)} %fusion.30, f32[1536,704]{0,1:T(8,128)} %fusion.31, f32[704]{0:T(1024)S(1)} %get-tuple-element.10, f32[704]{0:T(1024)S(1)} %get-tuple-element.9, f32[704]{0:T(1024)S(1)} %get-tuple-element.8, f32[704]{0:T(1024)S(1)} %get-tuple-element.20, ...), kind=kOutput, calls=%fused_computation.9 | convolution fusion | flops 4453957632 | bytes 17842688 | tf_op jit(solution)/shard_map/dot_general | solution.py:112
  242.3 0.0 reduce-scatter.2.cloned.1.call-update
  242.3 55.4 %reduce-scatter.2.cloned.1.call-done = bf16[192,2048]{1,0:T(8,128)(2,1)} async-done(((bf16[1536,2048]{1,0:T(8,128)(2,1)}), bf16[192,2048]{1,0:T(8,128)(2,1)}) %reduce-scatter.2.cloned.1.call-update) | async-done | bytes 786448 | tf_op jit(solution)/shard_map/reduce_scatter | solution.py:111
  297.7 1.4 fusion.49
  299.1 0.0 copy-done.7
  299.1 2.8 fusion.52
  (12 shorter events, 0.1 us)
Async XLA Ops:
  6.5 68.9 %all-gather.3.cloned.1.call-start = ((), (), s32[]{:S(2)}) async-start(), calls=%async_computation.3 | async-start | bytes 7077888 | tf_op jit(solution)/shard_map/all_gather | solution.py:91
  7.3 11.9 %copy-start.3 = (bf16[128,704]{0,1:T(8,128)(2,1)S(1)}, bf16[128,704]{0,1:T(8,128)(2,1)}, u32[]{:S(2)}) copy-start(bf16[128,704]{0,1:T(8,128)(2,1)} %param.17) | copy-start | bytes 540676
  7.3 11.9 %copy-start.4 = (bf16[128,704]{0,1:T(8,128)(2,1)S(1)}, bf16[128,704]{0,1:T(8,128)(2,1)}, u32[]{:S(2)}) copy-start(bf16[128,704]{0,1:T(8,128)(2,1)} %param.16) | copy-start | bytes 540676
  9.8 50.8 %copy-start.5 = (bf16[704,128]{1,0:T(8,128)(2,1)S(1)}, bf16[704,128]{1,0:T(8,128)(2,1)}, u32[]{:S(2)}) copy-start(bf16[704,128]{1,0:T(8,128)(2,1)} %param.20) | copy-start | bytes 540676
  9.8 50.8 %all-to-all-start = ((bf16[16,4,32,512]{3,2,1,0:T(8,128)(2,1)}), bf16[16,4,32,512]{3,2,1,0:T(8,128)(2,1)S(1)}, u32[]{:S(2)}, u32[]{:S(2)}) async-start(bf16[16,4,32,512]{3,2,1,0:T(8,128)(2,1)} %broadcast_in_dim.4), calls=%async_computation | async-start | bytes 4194304 | tf_op jit(solution)/shard_map/all_to_all | solution.py:12
  19.1 182.5 %all-gather.5.cloned.1.call-start = ((), (), s32[]{:S(2)}) async-start(), calls=%async_computation.4 | async-start | bytes 6127616 | tf_op jit(solution)/shard_map/all_gather | solution.py:32
  62.8 157.8 %all-to-all-start.1 = ((bf16[16,704,128]{2,1,0:T(8,128)(2,1)}), bf16[16,704,128]{2,1,0:T(8,128)(2,1)}, u32[]{:S(2)}, u32[]{:S(2)}) async-start(bf16[16,704,128]{2,1,0:T(8,128)(2,1)} %broadcast_in_dim.5), calls=%async_computation.1 | async-start | bytes 5767168 | tf_op jit(solution)/shard_map/all_to_all | solution.py:12
  73.9 223.9 %reduce-scatter.2.cloned.1.call-start = ((), (), s32[]{:S(2)}) async-start(), calls=%async_computation.5 | async-start | bytes 7077888 | tf_op jit(solution)/shard_map/reduce_scatter | solution.py:111
  75.4 4.2 %copy-start.6 = (f32[2048]{0:T(1024)S(1)}, f32[2048]{0:T(1024)}, u32[]{:S(2)}) copy-start(f32[2048]{0:T(1024)} %param.12) | copy-start | bytes 24580
  75.4 4.6 %copy-start = (bf16[1536,2048]{1,0:T(8,128)(2,1)S(1)}, bf16[1536,2048]{1,0:T(8,128)(2,1)}, u32[]{:S(2)}) copy-start(bf16[1536,2048]{1,0:T(8,128)(2,1)} %all-gather.3.cloned.1.call-done) | copy-start | bytes 18874372
  94.0 6.2 %copy-start.2 = (bf16[16,4,32,512]{3,2,0,1:T(8,128)(2,1)S(1)}, bf16[16,4,32,512]{3,2,0,1:T(8,128)(2,1)}, u32[]{:S(2)}) copy-start(bf16[16,4,32,512]{3,2,0,1:T(8,128)(2,1)} %copy.16) | copy-start | bytes 6291460
  107.9 12.6 %copy-start.8 = (f32[2048]{0:T(1024)S(1)}, f32[2048]{0:T(1024)}, u32[]{:S(2)}) copy-start(f32[2048]{0:T(1024)} %param.14) | copy-start | bytes 24580
  120.5 81.1 %copy-start.10 = (f32[2048]{0:T(1024)S(1)}, f32[2048]{0:T(1024)}, u32[]{:S(2)}) copy-start(f32[2048]{0:T(1024)} %param.15) | copy-start | bytes 24580
  201.6 12.3 %copy-start.1 = (f32[1536,2048]{1,0:T(8,128)S(1)}, f32[1536,2048]{1,0:T(8,128)}, u32[]{:S(2)}) copy-start(f32[1536,2048]{1,0:T(8,128)} %get-tuple-element.12) | copy-start | bytes 37748740
  201.6 12.3 %copy-start.9 = (bf16[2048,1408]{0,1:T(8,128)(2,1)S(1)}, bf16[2048,1408]{0,1:T(8,128)(2,1)}, u32[]{:S(2)}) copy-start(bf16[2048,1408]{0,1:T(8,128)(2,1)} %all-gather.5.cloned.1.call-done) | copy-start | bytes 17301508
  242.3 56.8 %copy-start.7 = (f32[2048]{0:T(1024)S(1)}, f32[2048]{0:T(1024)}, u32[]{:S(2)}) copy-start(f32[2048]{0:T(1024)} %param.21) | copy-start | bytes 24580
Sparse Core Ops, SparseCore 0:
  9.2 47.5 all-gather.2
  58.5 143.1 all-gather.4
  242.4 55.2 reduce-scatter.1
where the time goes:
time: 309 us; the launch traced here: 308 us
  waiting for transfers between devices  164 us (53%)
  matrix products  48.3 us (16%)
  other arithmetic  42.1 us (14%)
  starting transfers between devices  20.4 us (7%)
  local copies, waits for them, and re-layouts  20.2 us (7%)
  between operations  13.3 us (4%)
    all_gather x1, waiting for transfers between devices, sent_together(): lax.all_gather(both, axis, axis=dim, tiled=True)  68.4 us
    reduce_scatter x1, waiting for transfers between devices, shards(): lax.psum_scatter(jnp.dot(hidden, down_full, preferred_element_type=jnp.fl...  55.4 us
    all_to_all x2, waiting for transfers between devices, sent_to_all(): return lax.all_to_all(copies, axis, split_axis=0, concat_axis=0, tiled=True)  39.6 us
    dot_general x1, matrix products, shards(): jnp.dot(hidden, down_full, preferred_element_type=jnp.float32)  21.6 us
    all_to_all x2, starting transfers between devices, sent_to_all(): return lax.all_to_all(copies, axis, split_axis=0, concat_axis=0, tiled=True)  20.3 us
    reduce_sum x3, other arithmetic, rms_scale(): jnp.mean(floats * floats, axis=-1, keepdims=True) + rms_eps  18.3 us
    convert_element_type x1, local copies, waits for them, and re-layouts, rms_scale(): floats = values.astype(jnp.float32)  12.6 us
    dot_general x1, matrix products, shards(): gate_part = jnp.dot(whole, pieces[0], preferred_element_type=jnp.float32)  12.3 us
  transfers between devices with their start and end apart: 5, of which 3 were waited for; matrix products, arithmetic and copies ran while one was open for 27% of the time, Pallas kernels for 0%

commit v1 on v0

v1 whole, which is shorter than its diff:
```python
import functools

import jax
import jax.numpy as jnp
from jax import lax
from jax.experimental import pallas as pl
from jax.experimental.pallas import tpu as pltpu
from jax.sharding import PartitionSpec as P

MESH = pl.DeviceIdType.MESH
eps = 1e-06
ROWS = 192
HALO = 32
EXT = ROWS + HALO
OUTR = ROWS + 16
D = 2048
W = 704
WP = 768
GW = 2 * W
MAIN = 640
LANES = 128


def ring(value, n):
    return lax.rem(value + n, n)


class Gather:
    def __init__(self, piece, bundle, other, p, s, devs, partner, ssem, rsem):
        self.piece, self.bundle, self.other = piece, bundle, other
        self.p, self.s = p, s
        self.pu, self.pd, self.su, self.sd = devs
        self.partner = partner
        self.ssem, self.rsem = ssem, rsem
        self.sent = []

    def send(self, ref, dev, k):
        copy = pltpu.make_async_remote_copy(ref, ref, self.ssem.at[k], self.rsem.at[k], device_id=dev, device_id_type=MESH)
        copy.start()
        self.sent.append(copy)

    def recv(self, ref, k):
        pltpu.make_async_remote_copy(
            ref, ref, self.ssem.at[k], self.rsem.at[k], device_id=self.partner, device_id_type=MESH
        ).wait_recv()

    def s1(self):
        own = self.piece(self.p, None)
        self.send(own, self.pu, 0)
        self.send(own, self.pd, 1)

    def s2(self):
        low, high = ring(self.p - 1, 4), ring(self.p + 1, 4)
        self.recv(self.piece(low, None), 0)
        self.send(self.piece(low, 0), self.pu, 2)
        self.recv(self.piece(high, None), 1)
        self.send(self.piece(high, 1), self.pd, 3)

    def s3(self):
        far = ring(self.p + 2, 4)
        self.recv(self.piece(far, 0), 2)
        self.recv(self.piece(far, 1), 3)
        own = self.bundle(self.s, None)
        self.send(own, self.su, 4)
        self.send(own, self.sd, 5)
        self.send(own, self.partner, 8)

    def s4(self):
        low, high = ring(self.s - 1, 4), ring(self.s + 1, 4)
        self.recv(self.bundle(low, None), 4)
        self.send(self.bundle(low, 0), self.su, 6)
        self.recv(self.bundle(high, None), 5)
        self.send(self.bundle(high, 1), self.sd, 7)
        self.send(self.bundle(low, None), self.partner, 9)
        self.send(self.bundle(high, None), self.partner, 10)

    def s5(self):
        far = ring(self.s + 2, 4)
        self.recv(self.bundle(far, 0), 6)
        self.recv(self.bundle(far, 1), 7)
        self.send(self.bundle(far, None), self.partner, 11)

    def join(self):
        for k, off in ((8, 0), (9, -1), (10, 1), (11, 2)):
            self.recv(self.other(ring(self.s + off, 4)), k)

    def drain(self):
        for copy in self.sent:
            copy.wait_send()


def layer(
    tokens, pool_w, gu_w, dn_w, taps, gains, out,
    XB, NB, GAP, MIX, POOL, GU, DN, X, PRE, HID, SB, RB, R, AM,
    loc_sem, g_ssem, g_rsem, x_ssem, x_rsem, barrier_unused=None,
):
    rep, fs, tp = lax.axis_index("rep"), lax.axis_index("fs"), lax.axis_index("tp")
    zl, y = lax.div(fs, 4), lax.rem(fs, 4)
    z = rep * 4 + zl
    x, c = lax.div(tp, 2), lax.rem(tp, 2)

    def at_y(d):
        return (rep, zl * 4 + ring(y + d, 4), tp)

    def at_z(d):
        zn = ring(z + d, 8)
        return (lax.div(zn, 4), lax.rem(zn, 4) * 4 + y, tp)

    def at_tp(t):
        return (rep, fs, t)

    partner = at_tp(x * 2 + (1 - c))
    x_up, x_down = at_tp(ring(x + 1, 4) * 2 + c), at_tp(ring(x - 1, 4) * 2 + c)
    after = at_tp(ring(tp + 1, 8))
    cross = at_tp(ring(tp + 2 * c - 1, 8))
    y_up, y_down, z_up, z_down = at_y(1), at_y(-1), at_z(1), at_z(-1)

    mine = pl.ds(pl.multiple_of(c * GW, LANES), GW)
    theirs = pl.ds(pl.multiple_of((1 - c) * GW, LANES), GW)
    local = [
        pltpu.make_async_copy(tokens, XB.at[x, pl.ds(HALO, ROWS)], loc_sem.at[0]),
        pltpu.make_async_copy(pool_w.at[pl.ds(c * 2, 2)], POOL.at[pl.ds(c * 2, 2), zl, y], loc_sem.at[1]),
        pltpu.make_async_copy(gu_w, GU.at[zl, y, :, mine], loc_sem.at[2]),
        pltpu.make_async_copy(dn_w, DN.at[c, zl, y, pl.ds(0, W)], loc_sem.at[3]),
    ]
    for copy in local:
        copy.start()

    barrier = pltpu.get_barrier_semaphore()
    greeted = (partner, x_up, x_down, cross, y_up, y_down, z_up, z_down)
    for dev in greeted:
        pl.semaphore_signal(barrier, inc=1, device_id=dev, device_id_type=MESH)
    DN[:, :, :, W:WP, :] = jnp.zeros((2, 4, 4, WP - W, LANES), jnp.bfloat16)
    pl.semaphore_wait(barrier, len(greeted))
    for copy in local:
        copy.wait()

    def gathers(piece_a, bundle_a, other_a, piece_b, bundle_b, other_b, n):
        yz = (y_up, y_down, z_up, z_down)
        zy = (z_up, z_down, y_up, y_down)
        return (
            Gather(piece_a, bundle_a, other_a, y, zl, yz, partner, g_ssem.at[n], g_rsem.at[n]),
            Gather(piece_b, bundle_b, other_b, zl, y, zy, partner, g_ssem.at[n + 1], g_rsem.at[n + 1]),
        )

    def cut(start, size, sub):
        return pl.ds(start, size) if sub is None else pl.ds(start + sub * (size // 2), size // 2)

    pool = gathers(
        lambda p, sub: POOL.at[2 * c, zl, p, cut(0, 32, sub)],
        lambda s, sub: POOL.at[2 * c, s, :, cut(0, 32, sub)],
        lambda s: POOL.at[2 * (1 - c), s],
        lambda p, sub: POOL.at[2 * c + 1, p, y, cut(0, 32, sub)],
        lambda s, sub: POOL.at[2 * c + 1, :, s, cut(0, 32, sub)],
        lambda s: POOL.at[2 * (1 - c) + 1, :, s],
        0,
    )
    gu = gathers(
        lambda p, sub: GU.at[zl, p, cut(0, 64, sub), mine],
        lambda s, sub: GU.at[s, :, cut(0, 64, sub), mine],
        lambda s: GU.at[s, :, pl.ds(0, 64), theirs],
        lambda p, sub: GU.at[p, y, cut(64, 64, sub), mine],
        lambda s, sub: GU.at[:, s, cut(64, 64, sub), mine],
        lambda s: GU.at[:, s, pl.ds(64, 64), theirs],
        2,
    )
    dn = gathers(
        lambda p, sub: DN.at[c, zl, p, cut(0, 352, sub)],
        lambda s, sub: DN.at[c, s, :, cut(0, 352, sub)],
        lambda s: DN.at[1 - c, s, :, pl.ds(0, 352)],
        lambda p, sub: DN.at[c, p, y, cut(352, 352, sub)],
        lambda s, sub: DN.at[c, :, s, cut(352, 352, sub)],
        lambda s: DN.at[1 - c, :, s, pl.ds(352, 352)],
        4,
    )

    sent = []

    def push(src, dst, k, dev):
        copy = pltpu.make_async_remote_copy(src, dst, x_ssem.at[k], x_rsem.at[k], device_id=dev, device_id_type=MESH)
        copy.start()
        sent.append(copy)

    def arrived(dst, k):
        pltpu.make_async_remote_copy(
            dst, dst, x_ssem.at[k], x_rsem.at[k], device_id=partner, device_id_type=MESH
        ).wait_recv()

    low, high, far = ring(x - 1, 4), ring(x + 1, 4), ring(x + 2, 4)
    body = pl.ds(HALO, ROWS)
    head, tail = pl.ds(HALO, 96), pl.ds(HALO + 96, 96)
    last = pl.ds(EXT - HALO, HALO)
    top = pl.ds(0, HALO)

    push(XB.at[x, last], XB.at[ring(x + c, 4), top], 4, after)
    for g in pool:
        g.s1()
    push(XB.at[x, body], XB.at[x, body], 0, x_up)
    push(XB.at[x, body], XB.at[x, body], 1, x_down)
    for g in gu:
        g.s1()

    def side(m, slot):
        push(XB.at[ring(x + 1 - c + m, 4), last], XB.at[slot, top], 5 + m, partner)

    def mix(b, first_row, own):
        at_start = jnp.where(first_row == 0, 0.0, 1.0)
        XB[b, 0:HALO] = (XB[b, 0:HALO].astype(jnp.float32) * at_start).astype(jnp.bfloat16)

        def norm(i, _):
            r = pl.ds(pl.multiple_of(i * 16, 16), 16)
            v = XB[b, r, :].astype(jnp.float32)
            scale = lax.rsqrt(jnp.mean(v * v, axis=-1, keepdims=True) + eps)
            NB[r, :] = (v * scale * gains[0:1, :]).astype(jnp.bfloat16).astype(jnp.float32)
            return 0

        lax.fori_loop(0, EXT // 16, norm, 0)

        def pooled(i, _):
            r = pl.ds(pl.multiple_of(i * 16, 16), 16)
            both = pl.ds(pl.multiple_of(i * 16, 16), 32)
            where = first_row + i * 16 - 16 + lax.broadcasted_iota(jnp.int32, (16, LANES), 0)
            for g in range(4):
                span = 2 << g
                block = NB[both, g * 512:(g + 1) * 512]
                total = block
                for k in range(g + 1):
                    total = total + pltpu.roll(total, 1 << k, 0)
                inverse = 1.0 / jnp.clip(where + 1, 1, span).astype(jnp.float32)
                inverse = jnp.concatenate([inverse] * 4, axis=1)
                GAP[r, g * 512:(g + 1) * 512] = (total[16:] * inverse - block[16:]).astype(jnp.bfloat16)
            return 0

        lax.fori_loop(0, OUTR // 16, pooled, 0)
        for g in range(4):
            cols = slice(g * 512, (g + 1) * 512)
            MIX[:, cols] = jnp.dot(
                GAP[:, cols], POOL[g].reshape(512, 512), preferred_element_type=jnp.float32
            ).astype(jnp.bfloat16)

        def finish(i, _):
            r = pl.ds(pl.multiple_of(i * 16, 16), 16)
            v = MIX[r, :].astype(jnp.float32)
            scale = lax.rsqrt(jnp.mean(v * v, axis=-1, keepdims=True) + eps)
            t = XB[b, pl.ds(pl.multiple_of(i * 16 + 16, 16), 16), :].astype(jnp.float32)
            a = t + v * scale * gains[1:2, :]
            if own:
                AM[r, :] = a
            scale = lax.rsqrt(jnp.mean(a * a, axis=-1, keepdims=True) + eps)
            X[b, r, :] = (a * scale * gains[2:3, :]).astype(jnp.bfloat16)
            return 0

        lax.fori_loop(0, OUTR // 16, finish, 0)

    def start_of(b):
        return (2 * b + c) * ROWS

    for g in pool:
        g.s2()
    for g in pool:
        g.s3()
    for g in gu:
        g.s2()
    for g in pool:
        g.s4()
    for g in gu:
        g.s3()
    for g in pool:
        g.s5()
    for g in dn:
        g.s1()
    for g in pool:
        g.join()
    arrived(XB.at[x, top], 4)
    mix(x, start_of(x), True)
    for g in dn:
        g.s2()
    arrived(XB.at[low, body], 0)
    push(XB.at[low, head], XB.at[low, head], 2, x_up)
    arrived(XB.at[high, body], 1)
    push(XB.at[high, tail], XB.at[high, tail], 3, x_down)
    side(0, high)
    arrived(XB.at[high, top], 5)
    mix(high, start_of(high), False)
    for g in gu:
        g.s4()
    for g in dn:
        g.s3()
    arrived(XB.at[far, head], 2)
    arrived(XB.at[far, tail], 3)
    side(1, far)
    side(2, low)
    arrived(XB.at[far, top], 6)
    mix(far, start_of(far), False)
    arrived(XB.at[low, top], 7)
    mix(low, start_of(low), False)
    for g in gu:
        g.s5()
    for g in gu:
        g.join()

    def hidden_of(q, _):
        b = ring(x + 2 + q, 4)

        def project(j, _):
            cols = pl.ds(pl.multiple_of(j * 256, 256), 256)
            w = GU[:, :, :, cols].reshape(D, 256)
            PRE[:, cols] = jnp.dot(X[b], w, preferred_element_type=jnp.float32).astype(jnp.bfloat16).astype(jnp.float32)
            return 0

        lax.fori_loop(0, 2 * GW // 256, project, 0)

        def conv(first, taps_at, base, row):
            total = None
            for k in range(3):
                v = PRE[14 + row + k:14 + row + k + 48, pl.ds(first, LANES)]
                term = taps[base + k:base + k + 1, pl.ds(taps_at, LANES)] * v
                total = term if total is None else total + term
            return total

        def act(gate, up):
            inner = 0.7978845608028654 * (gate + 0.044715 * gate * gate * gate)
            return 0.5 * gate * (1.0 + jnp.tanh(inner)) * up

        for h in range(2):
            def main(t, _):
                to = pl.multiple_of(t * LANES, LANES)
                for row in range(0, ROWS, 48):
                    gate = conv(pl.multiple_of(h * GW + to, LANES), pl.multiple_of(h * WP + to, LANES), 0, row)
                    up = conv(pl.multiple_of(h * GW + MAIN + to, LANES), pl.multiple_of(h * WP + to, LANES), 3, row)
                    HID[b, h, row:row + 48, pl.ds(to, LANES)] = act(gate, up).astype(jnp.bfloat16)
                return 0

            lax.fori_loop(0, MAIN // LANES, main, 0)
            inside = lax.broadcasted_iota(jnp.int32, (48, LANES), 1) < 64
            for row in range(0, ROWS, 48):
                gate = conv(h * GW + 2 * MAIN, h * WP + MAIN, 0, row)
                up = pltpu.roll(conv(h * GW + 2 * MAIN, h * WP + MAIN, 3, row), 64, 1)
                HID[b, h, row:row + 48, MAIN:WP] = jnp.where(inside, act(gate, up), 0.0).astype(jnp.bfloat16)
        return 0

    lax.fori_loop(0, 1, hidden_of, 0)
    for g in dn:
        g.s4()
    lax.fori_loop(1, 4, hidden_of, 0)
    for g in dn:
        g.s5()
    for g in dn:
        g.join()

    def down(b):
        def part(j, _):
            total = None
            zz, yy = lax.div(j, 2), lax.rem(j, 2) * 2
            for h in range(2):
                w = jnp.concatenate([DN[h, zz, yy], DN[h, zz, yy + 1]], axis=1)
                term = jnp.dot(HID[b, h], w, preferred_element_type=jnp.float32)
                total = term if total is None else total + term
            SB[b, :, pl.ds(pl.multiple_of(j * 256, 256), 256)] = total.astype(jnp.bfloat16)
            return 0

        lax.fori_loop(0, 8, part, 0)

    def relay(b, start, k):
        def add(i, _):
            r = pl.ds(pl.multiple_of(start + i * 16, 16), 16)
            q = pl.ds(pl.multiple_of(i * 16, 16), 16)
            SB[b, r, :] = (SB[b, r, :].astype(jnp.float32) + RB[k, q, :].astype(jnp.float32)).astype(jnp.bfloat16)
            return 0

        lax.fori_loop(0, 6, add, 0)

    first, second = pl.ds(0, 96), pl.ds(96, 96)
    down(far)
    push(SB.at[far, first], RB.at[0], 8, x_up)
    push(SB.at[far, second], RB.at[1], 9, x_down)
    down(high)
    push(SB.at[high, second], R.at[0, second], 10, x_up)
    down(low)
    push(SB.at[low, first], R.at[1, first], 11, x_down)
    down(x)
    arrived(RB.at[0], 8)
    relay(high, 0, 0)
    push(SB.at[high, first], R.at[0, first], 12, x_up)
    arrived(RB.at[1], 9)
    relay(low, 96, 1)
    push(SB.at[low, second], R.at[1, second], 13, x_down)

    def last_rows(i, _):
        r = pl.ds(pl.multiple_of(i * 16, 16), 16)
        v = SB[x, r, :].astype(jnp.float32) + R[0, r, :].astype(jnp.float32) + R[1, r, :].astype(jnp.float32)
        scale = lax.rsqrt(jnp.mean(v * v, axis=-1, keepdims=True) + eps)
        a = AM[pl.ds(pl.multiple_of(i * 16 + 16, 16), 16), :]
        out[r, :] = (a + v * scale * gains[3:4, :]).astype(jnp.bfloat16)
        return 0

    arrived(R.at[0, second], 10)
    arrived(R.at[1, first], 11)
    arrived(R.at[0, first], 12)
    arrived(R.at[1, second], 13)
    lax.fori_loop(0, ROWS // 16, last_rows, 0)
    for copy in sent:
        copy.wait_send()
    for pair in (pool, gu, dn):
        for g in pair:
            g.drain()


def shards(
    tokens,
    mix_gain_in,
    pool_weight,
    mix_gain_out,
    ffn_gain_in,
    gate_weight,
    up_weight,
    gate_taps,
    up_taps,
    down_weight,
    ffn_gain_out,
):
    x = lax.axis_index("tp") // 2
    gu = jnp.concatenate(
        [gate_weight[:, :MAIN], up_weight[:, :MAIN], gate_weight[:, MAIN:], up_weight[:, MAIN:]], axis=1
    )
    gate_own = lax.dynamic_slice_in_dim(gate_taps, x * GW, GW, 1).reshape(3, 2, W)
    up_own = lax.dynamic_slice_in_dim(up_taps, x * GW, GW, 1).reshape(3, 2, W)
    blank = jnp.zeros((3, 2, WP - W), jnp.float32)
    gate_own = jnp.concatenate([gate_own, blank], axis=2)
    up_own = jnp.concatenate([up_own[:, :, :MAIN], blank, up_own[:, :, MAIN:]], axis=2)
    taps = jnp.pad(jnp.concatenate([gate_own, up_own], axis=0), ((0, 2), (0, 0), (0, 0))).reshape(8, 2 * WP)
    gains = jnp.stack([mix_gain_in, mix_gain_out, ffn_gain_in, ffn_gain_out])
    anywhere = pl.BlockSpec(memory_space=pl.ANY)
    vmem = pl.BlockSpec(memory_space=pltpu.VMEM)
    bf16, f32 = jnp.bfloat16, jnp.float32
    return pl.pallas_call(
        layer,
        out_shape=jax.ShapeDtypeStruct((ROWS, D), bf16),
        in_specs=[anywhere, anywhere, anywhere, anywhere, vmem, vmem],
        out_specs=vmem,
        scratch_shapes=[
            pltpu.VMEM((4, EXT, D), bf16),
            pltpu.VMEM((EXT, D), f32),
            pltpu.VMEM((OUTR, D), bf16),
            pltpu.VMEM((OUTR, D), bf16),
            pltpu.VMEM((4, 4, 4, 32, 512), bf16),
            pltpu.VMEM((4, 4, 128, 2 * GW), bf16),
            pltpu.VMEM((2, 4, 4, WP, LANES), bf16),
            pltpu.VMEM((4, OUTR, D), bf16),
            pltpu.VMEM((OUTR, 2 * GW), f32),
            pltpu.VMEM((4, 2, ROWS, WP), bf16),
            pltpu.VMEM((4, ROWS, D), bf16),
            pltpu.VMEM((2, 96, D), bf16),
            pltpu.VMEM((2, ROWS, D), bf16),
            pltpu.VMEM((OUTR, D), f32),
            pltpu.SemaphoreType.DMA((4,)),
            pltpu.SemaphoreType.DMA((6, 12)),
            pltpu.SemaphoreType.DMA((6, 12)),
            pltpu.SemaphoreType.DMA((14,)),
            pltpu.SemaphoreType.DMA((14,)),
        ],
        compiler_params=pltpu.CompilerParams(collective_id=0, has_side_effects=True, vmem_limit_bytes=60 * 1024 * 1024),
    )(tokens, pool_weight, gu, down_weight, taps, gains)


def solution(mesh):
    in_specs = (
        P(("rep", "fs", "tp"), None),
        P(),
        P(None, "fs", None),
        P(),
        P(),
        P("fs", "tp"),
        P("fs", "tp"),
        P(),
        P(),
        P("tp", "fs"),
        P(),
    )
    out_specs = P(("rep", "fs", "tp"), None)
    return jax.shard_map(shards, mesh=mesh, in_specs=in_specs, out_specs=out_specs, check_vma=False)
```

time: 309 us -> 141 us (0.46)
  waiting for transfers between devices: 164 us -> 0 us
  Pallas kernels: 0 us -> 130 us
  matrix products: 48.3 us -> 0 us
  other arithmetic: 42.1 us -> 0.72 us
  starting transfers between devices: 20.4 us -> 0 us
  between operations: 13.3 us -> 0.11 us
  local copies, waits for them, and re-layouts: 20.2 us -> 9.03 us
    pallas_call x0 -> x1, Pallas kernels: none -> 130 us  [shards(): pl.pallas_call(layer, out_shape=jax.ShapeDtypeStruct((ROWS, D), bf16), in...]
    all_gather x2 -> x0, waiting for transfers between devices: 68.4 us -> none  [the longest x1 68.4 us: sent_together(): lax.all_gather(both, axis, axis=dim, tiled=True)]
    reduce_scatter x1 -> x0, waiting for transfers between devices: 55.4 us -> none  [shards(): lax.psum_scatter(jnp.dot(hidden, down_full, preferred_element_type=jnp.fl...]
    dot_general x4 -> x0, matrix products: 48.3 us -> none  [the longest x1 21.6 us: shards(): jnp.dot(hidden, down_full, preferred_element_type=jnp.float32)]
    all_to_all x2 -> x0, waiting for transfers between devices: 39.6 us -> none  [sent_to_all(): return lax.all_to_all(copies, axis, split_axis=0, concat_axis=0, tiled=True)]
    all_to_all x2 -> x0, starting transfers between devices: 20.3 us -> none  [sent_to_all(): return lax.all_to_all(copies, axis, split_axis=0, concat_axis=0, tiled=True)]
    reduce_sum x3 -> x0, other arithmetic: 18.3 us -> none  [rms_scale(): jnp.mean(floats * floats, axis=-1, keepdims=True) + rms_eps]
    convert_element_type x1 -> x0, local copies, waits for them, and re-layouts: 12.6 us -> none  [rms_scale(): floats = values.astype(jnp.float32)]
  transfers between devices with their start and end apart: 5 -> 0, of which waited for: 3 -> 0; matrix products, arithmetic and copies ran while one was open for 27% -> 0% of each run, Pallas kernels for 0% -> 0%
where the time goes in v1:
time: 141 us; the launch traced here: 140 us
  Pallas kernels  130 us (92%)
  local copies, waits for them, and re-layouts  9.03 us (6%)
    pallas_call x1, Pallas kernels, shards(): pl.pallas_call(layer, out_shape=jax.ShapeDtypeStruct((ROWS, D), bf16), in...  130 us
    unnamed x15, local copies, waits for them, and re-layouts  3.97 us

profile of v1, /device:TPU:1, one launch (start us, length us, event | category | flops | bytes accessed | tf_op | source)
XLA Modules:
  0.0 140.1 jit_solution(13795583413815330137)
XLA Ops:
  0.0 0.0 slice-start
  0.0 0.7 slice-done
  0.7 0.1 copy.22
  0.8 0.0 slice-start.2
  0.8 0.7 slice-done.2
  1.6 0.0 copy-start.3
  1.6 0.1 copy.23
  1.7 0.0 copy-start
  1.7 0.0 copy-start.1
  1.7 0.0 copy-start.2
  1.7 0.5 copy-done.3
  2.3 0.1 copy-done
  2.4 0.0 copy-done.1
  2.4 0.0 copy-done.2
  2.4 0.6 pad_maximum_fusion.gains
  3.1 0.8 constant_dynamic-slice_fusion
  3.8 0.1 reshape.10
  3.9 0.1 reshape.9
  4.0 0.1 fusion
  4.1 0.6 copy.24
  4.8 0.0 slice-start.1
  4.8 0.9 slice-done.1
  5.7 0.2 copy.20
  5.8 0.0 slice-start.3
  5.9 0.9 slice-done.3
  6.8 0.2 copy.21
  6.9 0.8 concatenate.12.gu_w
  7.8 130.3 %shard_map.109 = bf16[192,2048]{1,0:T(8,128)(2,1)} custom-call(bf16[192,2048]{1,0:T(8,128)(2,1)} %tokens.1, bf16[4,32,512]{2,1,0:T(8,128)(2,1)} %pool_w.1, bf16[128,1408]{1,0:T(8,128)(2,1)} %concatenate.12.gu_w, bf16[704,128]{1,0:T(8,128)(2,1)} %dn_w.1, f32[8,1536]{1,0:T(8,128)} %bitcast.7, f32[4,2048]{1,0:T(4,128)} %pad_maximum_fusion.gains), custom_call_target="tpu_custom_call" | custom-call | tf_op jit(solution)/shard_map/pallas_call | solution.py:436
  138.0 2.1 %copy.26 = bf16[192,2048]{1,0:T(8,128)(2,1)} copy(bf16[192,2048]{1,0:T(8,128)(2,1)} %shard_map.109) | data formatting | bytes 1572864
  (5 shorter events, 0.0 us)
Async XLA Ops:
  0.0 0.7 slice-start
  0.8 0.7 slice-start.2
  1.6 0.7 copy-start.3
  1.7 0.7 copy-start
  1.7 0.7 copy-start.1
  1.7 0.7 copy-start.2
  4.8 0.9 slice-start.1
  5.8 0.9 slice-start.3

commit v2 on v0

v2 whole, which is shorter than its diff:
```python
import jax
import jax.numpy as jnp
from jax import lax
from jax.experimental import pallas as pl
from jax.experimental.pallas import tpu as pltpu
from jax.sharding import PartitionSpec as P

MESH = pl.DeviceIdType.MESH
eps = 1e-06
ROWS = 192
HALO = 32
EXT = ROWS + HALO
OUTR = ROWS + 16
D = 2048
W = 704
WP = 768
GW = 2 * W
MAIN = 640
LANES = 128


def ring(value, n):
    return lax.rem(value + n, n)


class Flow:
    def __init__(self, piece, bundle, block, other, p, s, devs, partner, ssem, rsem):
        self.piece, self.bundle, self.block, self.other = piece, bundle, block, other
        self.s = s
        self.columns = [ring(p + k, 4) for k in (0, -1, 1, 2)]
        self.pu, self.pd, self.su, self.sd, self.pfar, self.sfar = devs
        self.partner = partner
        self.ssem, self.rsem = ssem, rsem

    def send(self, ref, dev, k, n):
        pltpu.make_async_remote_copy(
            ref, ref, self.ssem.at[k], self.rsem.at[n], device_id=dev, device_id_type=MESH
        ).start()

    def seen(self, ref, k, n):
        return pltpu.make_async_remote_copy(
            ref, ref, self.ssem.at[k], self.rsem.at[n], device_id=self.partner, device_id_type=MESH
        )

    def recv(self, ref, n):
        self.seen(ref, 0, n).wait_recv()


class Direct(Flow):
    def spread(self, j):
        col = self.columns[j]
        ref = self.piece(col, self.s, None)
        self.send(ref, self.su, 1, 3)
        self.send(ref, self.sd, 1, 4)
        self.send(self.piece(col, self.s, 0), self.sfar[0], 1, 5)
        self.send(self.piece(col, self.s, 1), self.sfar[1], 1, 5)

    def start(self):
        col = self.columns[0]
        ref = self.piece(col, self.s, None)
        self.send(ref, self.pu, 0, 0)
        self.send(ref, self.pd, 0, 1)
        self.send(self.piece(col, self.s, 0), self.pfar[0], 0, 2)
        self.send(self.piece(col, self.s, 1), self.pfar[1], 0, 2)
        self.spread(0)

    def p(self):
        for j in (1, 2, 3):
            self.recv(self.piece(self.columns[j], self.s, None), j - 1)
            self.spread(j)
        self.send(self.bundle(self.s), self.partner, 2, 6)

    def r(self):
        for k, off in ((3, -1), (4, 1), (5, 2)):
            ref = self.bundle(ring(self.s + off, 4))
            self.recv(ref, k)
            self.send(ref, self.partner, 2, 6)

    def join(self):
        self.recv(self.other(None), 6)

    def drain(self):
        for k, (m, n) in enumerate(((1, 3), (3, 4), (4, 4))):
            self.seen(self.block(m, n), k, 0).wait_send()


class Relay(Flow):
    def __init__(self, *args, split):
        super().__init__(*args)
        self.split = split

    def start_p(self):
        own = self.piece(self.columns[0], self.s, None)
        self.send(own, self.pu, 0, 0)
        self.send(own, self.pd, 0, 1)

    def spread(self, j):
        ref = self.piece(self.columns[j], self.s, None)
        self.send(ref, self.su, 2, 3 + 2 * j)
        self.send(ref, self.sd, 2, 4 + 2 * j)

    def start_s(self):
        self.spread(0)

    def give(self, off, k):
        self.send(self.bundle(ring(self.s + off, 4)), self.partner, 4, 12 + k * self.split)

    def p1f(self):
        low, high = self.columns[1], self.columns[2]
        self.recv(self.piece(low, self.s, None), 0)
        self.send(self.piece(low, self.s, 0), self.pu, 1, 2)
        self.recv(self.piece(high, self.s, None), 1)
        self.send(self.piece(high, self.s, 1), self.pd, 1, 2)

    def p1s(self):
        self.spread(1)
        self.spread(2)

    def p2(self):
        self.recv(self.piece(self.columns[3], self.s, None), 2)
        self.spread(3)
        self.give(0, 0)

    def q(self, j):
        col = self.columns[j]
        low, high = ring(self.s - 1, 4), ring(self.s + 1, 4)
        self.recv(self.piece(col, low, None), 3 + 2 * j)
        self.send(self.piece(col, low, 0), self.su, 3, 11)
        self.recv(self.piece(col, high, None), 4 + 2 * j)
        self.send(self.piece(col, high, 1), self.sd, 3, 11)
        if j == 3:
            self.give(-1, 1)
            self.give(1, 2)

    def q0(self):
        self.q(0)

    def q1(self):
        self.q(1)

    def q2(self):
        self.q(2)

    def q3(self):
        self.q(3)

    def r(self):
        self.recv(self.bundle(ring(self.s + 2, 4)), 11)
        self.give(2, 3)

    def join(self):
        self.recv(self.other(None), 12)

    def join1(self):
        for k, off in ((0, 0), (1, -1), (2, 1)):
            self.recv(self.other(ring(self.s + off, 4)), 12 + k)

    def join2(self):
        self.recv(self.other(ring(self.s + 2, 4)), 15)

    def drain(self):
        for k, (m, n) in enumerate(((1, 2), (1, 1), (2, 4), (1, 4), (4, 4))):
            self.seen(self.block(m, n), k, 0).wait_send()


def layer(
    tokens, pool_w, gate_w, up_w, dn_w, gate_taps, up_taps, gain0, gain1, gain2, gain3, out,
    XB, SC, GAP, MIX, AF, POOL, GU, DN, X, P0, P1, HID, SB, RB, R, AM, TW, TG, TU, TAPS, GAINS,
    loc_sem, g_ssem, g_rsem, x_ssem, x_rsem,
):
    rep, fs, tp = lax.axis_index("rep"), lax.axis_index("fs"), lax.axis_index("tp")
    zl, y = lax.div(fs, 4), lax.rem(fs, 4)
    z = rep * 4 + zl
    x, c = lax.div(tp, 2), lax.rem(tp, 2)

    def at_y(d):
        return (rep, zl * 4 + ring(y + d, 4), tp)

    def at_z(d):
        zn = ring(z + d, 8)
        return (lax.div(zn, 4), lax.rem(zn, 4) * 4 + y, tp)

    def at_tp(t):
        return (rep, fs, t)

    partner = at_tp(x * 2 + (1 - c))
    x_up, x_down = at_tp(ring(x + 1, 4) * 2 + c), at_tp(ring(x - 1, 4) * 2 + c)
    after = at_tp(ring(tp + 1, 8))
    cross = at_tp(ring(tp + 2 * c - 1, 8))
    y_up, y_down, z_up, z_down = at_y(1), at_y(-1), at_z(1), at_z(-1)
    y_far, z_far = (at_y(2), at_y(2)), (at_z(2), at_z(-2))

    barrier = pltpu.get_barrier_semaphore()
    greeted = (partner, x_up, x_down, cross, y_up, y_down, z_up, z_down, y_far[0], *z_far)
    for dev in greeted:
        pl.semaphore_signal(barrier, inc=1, device_id=dev, device_id_type=MESH)

    def cut(start, size, sub):
        start, size = (start, size) if sub is None else (start + sub * (size // 2), size // 2)
        return pl.ds(start if isinstance(start, int) else pl.multiple_of(start, 16), size)

    mine = pl.ds(pl.multiple_of(c * GW, LANES), GW)
    theirs = pl.ds(pl.multiple_of((1 - c) * GW, LANES), GW)
    pairs = [
        (gate_w, TW.at[0]),
        (up_w, TW.at[1]),
        (tokens, XB.at[x, pl.ds(HALO, ROWS)]),
        (pool_w.at[pl.ds(c * 2, 2)], POOL.at[pl.ds(c * 2, 2), zl, y]),
        (dn_w.at[pl.ds(0, MAIN)], DN.at[zl, y, cut(c * WP, MAIN, None)]),
        (dn_w.at[pl.ds(MAIN, 64)], DN.at[zl, y, cut(MAIN + c * 64, 64, None)]),
        (gate_taps.at[:, pl.ds(pl.multiple_of(x * GW, LANES), GW)], TG),
        (up_taps.at[:, pl.ds(pl.multiple_of(x * GW, LANES), GW)], TU),
        (gain0, GAINS.at[0]),
        (gain1, GAINS.at[1]),
        (gain2, GAINS.at[2]),
        (gain3, GAINS.at[3]),
    ]
    local = [pltpu.make_async_copy(src, dst, loc_sem.at[k]) for k, (src, dst) in enumerate(pairs)]
    for copy in local:
        copy.start()
    for copy in local:
        copy.wait()
    turned = [TW[k].T for k in range(2)]
    for k in range(2):
        for t in range(5):
            at = pl.multiple_of(c * 1536 + t * 256 + k * LANES, LANES)
            GU[zl, y, :, pl.ds(at, LANES)] = turned[k][:, t * LANES:(t + 1) * LANES]
    ends = [w[:, MAIN:W] for w in turned]
    both = jnp.concatenate([ends[0], ends[1]], axis=1).astype(jnp.float32)
    swapped = jnp.concatenate([ends[1], ends[0]], axis=1).astype(jnp.float32)
    pick = jnp.where(c == 0, both, swapped)
    GU[zl, y, :, pl.ds(pl.multiple_of(1280 + c * LANES, LANES), LANES)] = pick.astype(jnp.bfloat16)
    for ref, base in ((TG, 0), (TU, 3)):
        v = ref[...]
        TAPS[base:base + 3, 0:MAIN] = v[:, 0:MAIN]
        TAPS[base:base + 3, MAIN:WP] = jnp.concatenate([v[:, MAIN:W], v[:, W + MAIN:GW]], axis=1)
        TAPS[base:base + 3, WP:GW] = v[:, W:W + MAIN]
    with jax.named_scope("barrier_wait"):
        pl.semaphore_wait(barrier, len(greeted))

    yz = (y_up, y_down, z_up, z_down, y_far, z_far)
    zy = (z_up, z_down, y_up, y_down, z_far, y_far)

    def region(ref, rows, cols=None):
        def at(i, j, sub=None):
            start, size = rows
            here = cut(start, size, sub)
            return ref.at[i, j, here] if cols is None else ref.at[i, j, here, cols]

        return at

    every = slice(None)

    def pair(make, mine_a, mine_b, theirs_a, theirs_b, n, **more):
        def block(at):
            return lambda m, k: at(pl.ds(0, m), pl.ds(0, k))

        return (
            make(
                lambda p, s, sub: mine_a(s, p, sub), lambda s: mine_a(s, every), block(mine_a),
                lambda s: theirs_a(every if s is None else s, every),
                y, zl, yz, partner, g_ssem.at[n], g_rsem.at[n], **more,
            ),
            make(
                lambda p, s, sub: mine_b(p, s, sub), lambda s: mine_b(every, s), block(mine_b),
                lambda s: theirs_b(every, every if s is None else s),
                zl, y, zy, partner, g_ssem.at[n + 1], g_rsem.at[n + 1], **more,
            ),
        )

    pool = pair(
        Direct,
        region(POOL.at[2 * c], (0, 32)), region(POOL.at[2 * c + 1], (0, 32)),
        region(POOL.at[2 * (1 - c)], (0, 32)), region(POOL.at[2 * (1 - c) + 1], (0, 32)),
        0,
    )
    gu = pair(
        Relay,
        region(GU, (0, 64), mine), region(GU, (64, 64), mine),
        region(GU, (0, 64), theirs), region(GU, (64, 64), theirs),
        2, split=0,
    )
    dn = pair(
        Relay,
        region(DN, (c * W, 352)), region(DN, (c * W + 352, 352)),
        region(DN, ((1 - c) * W, 352)), region(DN, ((1 - c) * W + 352, 352)),
        4, split=1,
    )

    def push(src, dst, k, dev):
        n = 0 if k < 4 else 1 if k < 8 else 2
        pltpu.make_async_remote_copy(
            src, dst, x_ssem.at[n], x_rsem.at[k], device_id=dev, device_id_type=MESH
        ).start()

    def pushed(ref, n):
        pltpu.make_async_remote_copy(
            ref, ref, x_ssem.at[n], x_rsem.at[0], device_id=partner, device_id_type=MESH
        ).wait_send()

    def arrived(dst, k):
        pltpu.make_async_remote_copy(
            dst, dst, x_ssem.at[0], x_rsem.at[k], device_id=partner, device_id_type=MESH
        ).wait_recv()

    low, high, far = ring(x - 1, 4), ring(x + 1, 4), ring(x + 2, 4)
    body = pl.ds(HALO, ROWS)
    head, tail = pl.ds(HALO, 96), pl.ds(HALO + 96, 96)
    last = pl.ds(EXT - HALO, HALO)
    top = pl.ds(0, HALO)

    def side(m, slot):
        push(XB.at[ring(x + 1 - c + m, 4), last], XB.at[slot, top], 5 + m, partner)

    def rows16(i):
        return pl.ds(pl.multiple_of(i * 16, 16), 16)

    def prep(b, first_row):
        at_start = jnp.where(first_row == 0, 0.0, 1.0)
        XB[b, 0:HALO] = (XB[b, 0:HALO].astype(jnp.float32) * at_start).astype(jnp.bfloat16)

        def scales(i, _):
            v = XB[b, rows16(i), :].astype(jnp.float32)
            scale = lax.rsqrt(jnp.mean(v * v, axis=-1, keepdims=True) + eps)
            SC[rows16(i), :] = jnp.broadcast_to(scale, (16, LANES))
            return 0

        lax.fori_loop(0, EXT // 16, scales, 0, unroll=7)
        where = first_row + lax.broadcasted_iota(jnp.int32, (16, LANES), 0)
        for g in range(4):
            span = 2 << g
            inverse = 1.0 / jnp.clip(where + 1, 1, span).astype(jnp.float32)

            def strip(t, _):
                cols = pl.ds(pl.multiple_of(g * 512 + t * LANES, LANES), LANES)
                v = XB[b, :, cols].astype(jnp.float32) * SC[...] * GAINS[0, :, cols]
                v = v.astype(jnp.bfloat16).astype(jnp.float32)
                total = v
                for k in range(g + 1):
                    total = total + pltpu.roll(total, 1 << k, 0)
                GAP[0:16, cols] = (total[16:32] * (1.0 / span) - v[16:32]).astype(jnp.bfloat16)
                GAP[16:32, cols] = (total[32:48] * inverse - v[32:48]).astype(jnp.bfloat16)
                GAP[32:OUTR, cols] = (total[48:] * (1.0 / span) - v[48:]).astype(jnp.bfloat16)
                return 0

            lax.fori_loop(0, 4, strip, 0)

    def post(b, keep):
        for g in range(4):
            cols = slice(g * 512, (g + 1) * 512)
            MIX[:, cols] = jnp.dot(
                GAP[:, cols], POOL[g].reshape(512, 512), preferred_element_type=jnp.float32
            ).astype(jnp.bfloat16)

        def scales(i, _):
            v = MIX[rows16(i), :].astype(jnp.float32)
            scale = lax.rsqrt(jnp.mean(v * v, axis=-1, keepdims=True) + eps)
            SC[rows16(i), :] = jnp.broadcast_to(scale, (16, LANES))
            return 0

        lax.fori_loop(0, OUTR // 16, scales, 0, unroll=13)

        def added(i, _):
            total = jnp.zeros((16, LANES), jnp.float32)
            scale = SC[rows16(i), :]
            for t in range(D // LANES):
                cols = slice(t * LANES, (t + 1) * LANES)
                v = MIX[rows16(i), cols].astype(jnp.float32)
                rows = pl.ds(pl.multiple_of(i * 16 + 16, 16), 16)
                a = XB[b, rows, cols].astype(jnp.float32) + v * scale * GAINS[1, :, cols]
                keep[rows16(i), cols] = a
                total = total + a * a
            scale = lax.rsqrt(jnp.sum(total, axis=-1, keepdims=True) * (1.0 / D) + eps)
            SC[rows16(i), :] = jnp.broadcast_to(scale, (16, LANES))
            return 0

        lax.fori_loop(0, OUTR // 16, added, 0)

        def scaled(i, _):
            scale = SC[rows16(i), :]
            for t in range(D // LANES):
                cols = slice(t * LANES, (t + 1) * LANES)
                X[b, rows16(i), cols] = (keep[rows16(i), cols] * scale * GAINS[2, :, cols]).astype(jnp.bfloat16)
            return 0

        lax.fori_loop(0, OUTR // 16, scaled, 0)

    def start_of(b):
        return (2 * b + c) * ROWS

    def hidden(b, begin, stop):
        def project(i, ref):
            w = GU[:, :, :, pl.ds(pl.multiple_of(i * 256, 256), 256)].reshape(D, 256)
            ref[...] = jnp.dot(X[b], w, preferred_element_type=jnp.float32).astype(jnp.bfloat16).astype(jnp.float32)

        def conv(v, taps_at, base):
            taps = TAPS[base:base + 3, pl.ds(taps_at, LANES)]
            return taps[0:1] * pltpu.roll(v, 2, 0) + taps[1:2] * pltpu.roll(v, 1, 0) + taps[2:3] * v

        def act(ref, i, ends):
            at = i * LANES if ends else pl.multiple_of(i * LANES, LANES)
            for row in (0, 96):
                gate, up = ref[row:row + 112, 0:LANES], ref[row:row + 112, LANES:]
                if ends:
                    lead = lax.broadcasted_iota(jnp.int32, (112, LANES), 1) < 64
                    gate, up = jnp.where(lead, gate, up), pltpu.roll(jnp.where(lead, up, gate), 64, 1)
                gate, up = conv(gate, at, 0)[16:], conv(up, at, 3)[16:]
                inner = 0.7978845608028654 * (gate + 0.044715 * gate * gate * gate)
                value = 0.5 * gate * (1.0 + jnp.tanh(inner)) * up
                HID[b, row:row + 96, pl.ds(at, LANES)] = value.astype(jnp.bfloat16)

        def order(i):
            return i + jnp.minimum(lax.div(i, 5), 1) - 6 * lax.div(i, 10)

        if begin == 0:
            project(0, P0)

        def two(i, _):
            project(order(2 * i + 1), P1)
            act(P0, order(2 * i), False)
            project(order(2 * i + 2), P0)
            act(P1, order(2 * i + 1), False)
            return 0

        lax.fori_loop(begin, stop, two, 0)
        if stop == 5:
            act(P0, 5, True)

    steps = [(0, 0), (0, 1), (0, -1), (1, 0), (-1, 0), (1, 1), (1, -1), (-1, 1)]
    steps += [(-1, -1), (2, 0), (2, 1), (2, -1), (0, 2), (1, 2), (-1, 2), (2, 2)]
    slots = [(ring(zl + dz, 4), ring(y + dy, 4)) for dz, dy in steps]

    def down(b, part):
        for k in range(8 * part, 8 * part + 8, 2):
            w = jnp.concatenate([DN[slots[k]], DN[slots[k + 1]]], axis=1)
            total = jnp.dot(HID[b], w, preferred_element_type=jnp.float32).astype(jnp.bfloat16)
            SB[b, k] = total[:, 0:LANES]
            SB[b, k + 1] = total[:, LANES:]

    def relay(b, start, k, part):
        rows = pl.ds(start, 96)

        def add(i, _):
            SB[b, i, rows] = (SB[b, i, rows].astype(jnp.float32) + RB[k, i].astype(jnp.float32)).astype(jnp.bfloat16)
            return 0

        lax.fori_loop(8 * part, 8 * part + 8, add, 0)

    first, second = pl.ds(0, 96), pl.ds(96, 96)
    push(XB.at[x, last], XB.at[ring(x + c, 4), top], 4, after)
    for g in pool:
        g.start()
    for g in gu:
        g.start_p()
    push(XB.at[x, body], XB.at[x, body], 0, x_up)
    push(XB.at[x, body], XB.at[x, body], 1, x_down)
    for g in pool:
        g.p()
    for g in gu:
        g.start_s()
    for g in gu:
        g.p1f()
    for g in gu:
        g.p1s()
    arrived(XB.at[x, top], 4)
    prep(x, start_of(x))
    for g in pool:
        g.r()
    for g in pool:
        g.join()
    post(x, AM)
    for g in gu:
        g.p2()
    for g in gu:
        g.q0()
    arrived(XB.at[low, body], 0)
    push(XB.at[low, head], XB.at[low, head], 2, x_up)
    arrived(XB.at[high, body], 1)
    push(XB.at[high, tail], XB.at[high, tail], 3, x_down)
    side(0, high)
    arrived(XB.at[high, top], 5)
    prep(high, start_of(high))
    post(high, AF)
    for g in gu:
        g.q1()
    for g in gu:
        g.q2()
    for g in dn:
        g.start_p()
    arrived(XB.at[far, head], 2)
    arrived(XB.at[far, tail], 3)
    side(1, far)
    side(2, low)
    arrived(XB.at[far, top], 6)
    for g in gu:
        g.q3()
    for g in dn:
        g.start_s()
    prep(far, start_of(far))
    post(far, AF)
    for g in dn:
        g.p1f()
    for g in dn:
        g.p1s()
    for g in gu:
        g.r()
    arrived(XB.at[low, top], 7)
    prep(low, start_of(low))
    for g in dn:
        g.p2()
    post(low, AF)
    for g in dn:
        g.q0()
    for g in gu:
        g.join()
    hidden(far, 0, 3)
    for g in dn:
        g.q1()
    for g in dn:
        g.q2()
    hidden(far, 3, 5)
    for g in dn:
        g.q3()
    hidden(high, 0, 3)
    for g in dn:
        g.join1()
    down(far, 0)
    push(SB.at[far, pl.ds(0, 8), first], RB.at[0, pl.ds(0, 8)], 8, x_up)
    push(SB.at[far, pl.ds(0, 8), second], RB.at[1, pl.ds(0, 8)], 9, x_down)
    for g in dn:
        g.r()
    hidden(high, 3, 5)
    for g in dn:
        g.join2()
    down(far, 1)
    push(SB.at[far, pl.ds(8, 8), first], RB.at[0, pl.ds(8, 8)], 14, x_up)
    push(SB.at[far, pl.ds(8, 8), second], RB.at[1, pl.ds(8, 8)], 15, x_down)
    down(high, 0)
    push(SB.at[high, pl.ds(0, 8), second], R.at[0, pl.ds(0, 8), second], 10, x_up)
    hidden(low, 0, 5)
    down(low, 0)
    push(SB.at[low, pl.ds(0, 8), first], R.at[1, pl.ds(0, 8), first], 11, x_down)
    down(high, 1)
    push(SB.at[high, pl.ds(8, 8), second], R.at[0, pl.ds(8, 8), second], 16, x_up)
    down(low, 1)
    push(SB.at[low, pl.ds(8, 8), first], R.at[1, pl.ds(8, 8), first], 17, x_down)
    arrived(RB.at[0, pl.ds(0, 8)], 8)
    relay(high, 0, 0, 0)
    push(SB.at[high, pl.ds(0, 8), first], R.at[0, pl.ds(0, 8), first], 12, x_up)
    arrived(RB.at[1, pl.ds(0, 8)], 9)
    relay(low, 96, 1, 0)
    push(SB.at[low, pl.ds(0, 8), second], R.at[1, pl.ds(0, 8), second], 13, x_down)
    arrived(RB.at[0, pl.ds(8, 8)], 14)
    relay(high, 0, 0, 1)
    push(SB.at[high, pl.ds(8, 8), first], R.at[0, pl.ds(8, 8), first], 18, x_up)
    arrived(RB.at[1, pl.ds(8, 8)], 15)
    relay(low, 96, 1, 1)
    push(SB.at[low, pl.ds(8, 8), second], R.at[1, pl.ds(8, 8), second], 19, x_down)
    hidden(x, 0, 5)
    down(x, 0)
    down(x, 1)

    def last_rows(i, _):
        r = rows16(i)
        total = jnp.zeros((16, LANES), jnp.float32)
        values = []
        for k in range(16):
            v = SB[x, k, r].astype(jnp.float32) + R[0, k, r].astype(jnp.float32) + R[1, k, r].astype(jnp.float32)
            values.append(v)
            total = total + v * v
        scale = lax.rsqrt(jnp.sum(total, axis=-1, keepdims=True) * (1.0 / D) + eps)
        for k in range(16):
            cols = pl.ds(pl.multiple_of((slots[k][0] * 4 + slots[k][1]) * LANES, LANES), LANES)
            a = AM[pl.ds(pl.multiple_of(i * 16 + 16, 16), 16), cols]
            out[r, cols] = (a + values[k] * scale * GAINS[3, :, cols]).astype(jnp.bfloat16)
        return 0

    arrived(R.at[0, pl.ds(0, 8), second], 10)
    arrived(R.at[1, pl.ds(0, 8), first], 11)
    arrived(R.at[0, pl.ds(0, 8), first], 12)
    arrived(R.at[1, pl.ds(0, 8), second], 13)
    arrived(R.at[0, pl.ds(8, 8), second], 16)
    arrived(R.at[1, pl.ds(8, 8), first], 17)
    arrived(R.at[0, pl.ds(8, 8), first], 18)
    arrived(R.at[1, pl.ds(8, 8), second], 19)
    lax.fori_loop(0, ROWS // 16, last_rows, 0, unroll=2)
    with jax.named_scope("drain"):
        pushed(XB.at[pl.ds(0, 3), pl.ds(0, ROWS)], 0)
        pushed(XB.at[0, pl.ds(0, 4 * HALO)], 1)
        pushed(SB.at[pl.ds(0, 3)], 2)
        for both in (pool, gu, dn):
            for g in both:
                g.drain()


def shards(
    tokens,
    mix_gain_in,
    pool_weight,
    mix_gain_out,
    ffn_gain_in,
    gate_weight,
    up_weight,
    gate_taps,
    up_taps,
    down_weight,
    ffn_gain_out,
):
    anywhere = pl.BlockSpec(memory_space=pl.ANY)
    vmem = pl.BlockSpec(memory_space=pltpu.VMEM)
    bf16, f32 = jnp.bfloat16, jnp.float32
    gains = [g.reshape(1, D) for g in (mix_gain_in, mix_gain_out, ffn_gain_in, ffn_gain_out)]
    return pl.pallas_call(
        layer,
        out_shape=jax.ShapeDtypeStruct((ROWS, D), bf16),
        in_specs=[anywhere] * 11,
        out_specs=vmem,
        scratch_shapes=[
            pltpu.VMEM((4, EXT, D), bf16),
            pltpu.VMEM((EXT, LANES), f32),
            pltpu.VMEM((OUTR, D), bf16),
            pltpu.VMEM((OUTR, D), bf16),
            pltpu.VMEM((OUTR, D), f32),
            pltpu.VMEM((4, 4, 4, 32, 512), bf16),
            pltpu.VMEM((4, 4, 128, 2 * GW), bf16),
            pltpu.VMEM((4, 4, GW, LANES), bf16),
            pltpu.VMEM((4, OUTR, D), bf16),
            pltpu.VMEM((OUTR, 256), f32),
            pltpu.VMEM((OUTR, 256), f32),
            pltpu.VMEM((4, ROWS, GW), bf16),
            pltpu.VMEM((4, 16, ROWS, LANES), bf16),
            pltpu.VMEM((2, 16, 96, LANES), bf16),
            pltpu.VMEM((2, 16, ROWS, LANES), bf16),
            pltpu.VMEM((OUTR, D), f32),
            pltpu.VMEM((2, W, LANES), bf16),
            pltpu.VMEM((3, GW), f32),
            pltpu.VMEM((3, GW), f32),
            pltpu.VMEM((8, GW), f32),
            pltpu.VMEM((4, 1, D), f32),
            pltpu.SemaphoreType.DMA((12,)),
            pltpu.SemaphoreType.DMA((6, 5)),
            pltpu.SemaphoreType.DMA((6, 16)),
            pltpu.SemaphoreType.DMA((3,)),
            pltpu.SemaphoreType.DMA((20,)),
        ],
        compiler_params=pltpu.CompilerParams(collective_id=0, has_side_effects=True, vmem_limit_bytes=60 * 1024 * 1024),
    )(tokens, pool_weight, gate_weight.T, up_weight.T, down_weight, gate_taps, up_taps, *gains)


def solution(mesh):
    in_specs = (
        P(("rep", "fs", "tp"), None),
        P(),
        P(None, "fs", None),
        P(),
        P(),
        P("fs", "tp"),
        P("fs", "tp"),
        P(),
        P(),
        P("tp", "fs"),
        P(),
    )
    out_specs = P(("rep", "fs", "tp"), None)
    return jax.shard_map(shards, mesh=mesh, in_specs=in_specs, out_specs=out_specs, check_vma=False)
```

time: 309 us -> 98 us (0.32)
  waiting for transfers between devices: 164 us -> 0 us
  Pallas kernels: 0 us -> 95.7 us
  matrix products: 48.3 us -> 0 us
  other arithmetic: 42.1 us -> 0 us
  starting transfers between devices: 20.4 us -> 0 us
  local copies, waits for them, and re-layouts: 20.2 us -> 2.09 us
  between operations: 13.3 us -> 0.01 us
    pallas_call x0 -> x1, Pallas kernels: none -> 95.7 us  [shards(): pl.pallas_call(layer, out_shape=jax.ShapeDtypeStruct((ROWS, D), bf16), in...]
    all_gather x2 -> x0, waiting for transfers between devices: 68.4 us -> none  [the longest x1 68.4 us: sent_together(): lax.all_gather(both, axis, axis=dim, tiled=True)]
    reduce_scatter x1 -> x0, waiting for transfers between devices: 55.4 us -> none  [shards(): lax.psum_scatter(jnp.dot(hidden, down_full, preferred_element_type=jnp.fl...]
    dot_general x4 -> x0, matrix products: 48.3 us -> none  [the longest x1 21.6 us: shards(): jnp.dot(hidden, down_full, preferred_element_type=jnp.float32)]
    all_to_all x2 -> x0, waiting for transfers between devices: 39.6 us -> none  [sent_to_all(): return lax.all_to_all(copies, axis, split_axis=0, concat_axis=0, tiled=True)]
    all_to_all x2 -> x0, starting transfers between devices: 20.3 us -> none  [sent_to_all(): return lax.all_to_all(copies, axis, split_axis=0, concat_axis=0, tiled=True)]
    reduce_sum x3 -> x0, other arithmetic: 18.3 us -> none  [rms_scale(): jnp.mean(floats * floats, axis=-1, keepdims=True) + rms_eps]
    convert_element_type x1 -> x0, local copies, waits for them, and re-layouts: 12.6 us -> none  [rms_scale(): floats = values.astype(jnp.float32)]
  transfers between devices with their start and end apart: 5 -> 0, of which waited for: 3 -> 0; matrix products, arithmetic and copies ran while one was open for 27% -> 0% of each run, Pallas kernels for 0% -> 0%
where the time goes in v2:
time: 98 us; the launch traced here: 97.8 us
  Pallas kernels  95.7 us (98%)
  local copies, waits for them, and re-layouts  2.09 us (2%)
    pallas_call x1, Pallas kernels, shards(): pl.pallas_call(layer, out_shape=jax.ShapeDtypeStruct((ROWS, D), bf16), in...  95.7 us
    unnamed x1, local copies, waits for them, and re-layouts  2.09 us

profile of v2, /device:TPU:1, one launch (start us, length us, event | category | flops | bytes accessed | tf_op | source)
XLA Modules:
  0.0 97.8 jit_solution(13974750537665597605)
XLA Ops:
  0.0 95.7 %shard_map.109 = bf16[192,2048]{1,0:T(8,128)(2,1)} custom-call(bf16[192,2048]{1,0:T(8,128)(2,1)} %tokens.1, bf16[4,32,512]{2,1,0:T(8,128)(2,1)} %pool_w.1, bf16[704,128]{1,0:T(8,128)(2,1)} %bitcast.6, bf16[704,128]{1,0:T(8,128)(2,1)} %bitcast.7, bf16[704,128]{1,0:T(8,128)(2,1)} %dn_w.1, f32[3,5632]{1,0:T(4,128)} %gate_taps.1, f32[3,5632]{1,0:T(4,128)} %up_taps.1, ...), custom_call_target="tpu_custom_call" | custom-call | tf_op jit(solution)/shard_map/pallas_call | solution.py:613
  95.8 2.1 %copy.13 = bf16[192,2048]{1,0:T(8,128)(2,1)} copy(bf16[192,2048]{1,0:T(8,128)(2,1)} %shard_map.109) | data formatting | bytes 1572864

commit v3 on v2

--- a/solution.py
+++ b/solution.py
@@ -28,7 +28,7 @@
         self.piece, self.bundle, self.block, self.other = piece, bundle, block, other
         self.s = s
         self.columns = [ring(p + k, 4) for k in (0, -1, 1, 2)]
-        self.pu, self.pd, self.su, self.sd, self.pfar, self.sfar = devs
+        self.pu, self.pd, self.su, self.sd = devs
         self.partner = partner
         self.ssem, self.rsem = ssem, rsem
 
@@ -44,44 +44,6 @@
 
     def recv(self, ref, n):
         self.seen(ref, 0, n).wait_recv()
-
-
-class Direct(Flow):
-    def spread(self, j):
-        col = self.columns[j]
-        ref = self.piece(col, self.s, None)
-        self.send(ref, self.su, 1, 3)
-        self.send(ref, self.sd, 1, 4)
-        self.send(self.piece(col, self.s, 0), self.sfar[0], 1, 5)
-        self.send(self.piece(col, self.s, 1), self.sfar[1], 1, 5)
-
-    def start(self):
-        col = self.columns[0]
-        ref = self.piece(col, self.s, None)
-        self.send(ref, self.pu, 0, 0)
-        self.send(ref, self.pd, 0, 1)
-        self.send(self.piece(col, self.s, 0), self.pfar[0], 0, 2)
-        self.send(self.piece(col, self.s, 1), self.pfar[1], 0, 2)
-        self.spread(0)
-
-    def p(self):
-        for j in (1, 2, 3):
-            self.recv(self.piece(self.columns[j], self.s, None), j - 1)
-            self.spread(j)
-        self.send(self.bundle(self.s), self.partner, 2, 6)
-
-    def r(self):
-        for k, off in ((3, -1), (4, 1), (5, 2)):
-            ref = self.bundle(ring(self.s + off, 4))
-            self.recv(ref, k)
-            self.send(ref, self.partner, 2, 6)
-
-    def join(self):
-        self.recv(self.other(None), 6)
-
-    def drain(self):
-        for k, (m, n) in enumerate(((1, 3), (3, 4), (4, 4))):
-            self.seen(self.block(m, n), k, 0).wait_send()
 
 
 class Relay(Flow):
@@ -125,9 +87,9 @@
         col = self.columns[j]
         low, high = ring(self.s - 1, 4), ring(self.s + 1, 4)
         self.recv(self.piece(col, low, None), 3 + 2 * j)
-        self.send(self.piece(col, low, 0), self.su, 3, 11)
+        self.send(self.piece(col, low, 0), self.su, 3, self.landed(j))
         self.recv(self.piece(col, high, None), 4 + 2 * j)
-        self.send(self.piece(col, high, 1), self.sd, 3, 11)
+        self.send(self.piece(col, high, 1), self.sd, 3, self.landed(j))
         if j == 3:
             self.give(-1, 1)
             self.give(1, 2)
@@ -144,9 +106,20 @@
     def q3(self):
         self.q(3)
 
-    def r(self):
-        self.recv(self.bundle(ring(self.s + 2, 4)), 11)
-        self.give(2, 3)
+    def landed(self, j):
+        return 11 if j == 0 else 15 + j
+
+    def far(self, j):
+        ref = self.piece(self.columns[j], ring(self.s + 2, 4), None)
+        self.recv(ref, self.landed(j))
+        self.send(ref, self.partner, 4, 12 + 3 * self.split)
+
+    def r012(self):
+        for j in range(3):
+            self.far(j)
+
+    def r3(self):
+        self.far(3)
 
     def join(self):
         self.recv(self.other(None), 12)
@@ -188,10 +161,9 @@
     after = at_tp(ring(tp + 1, 8))
     cross = at_tp(ring(tp + 2 * c - 1, 8))
     y_up, y_down, z_up, z_down = at_y(1), at_y(-1), at_z(1), at_z(-1)
-    y_far, z_far = (at_y(2), at_y(2)), (at_z(2), at_z(-2))
 
     barrier = pltpu.get_barrier_semaphore()
-    greeted = (partner, x_up, x_down, cross, y_up, y_down, z_up, z_down, y_far[0], *z_far)
+    greeted = (partner, x_up, x_down, cross, y_up, y_down, z_up, z_down)
     for dev in greeted:
         pl.semaphore_signal(barrier, inc=1, device_id=dev, device_id_type=MESH)
 
@@ -218,28 +190,33 @@
     local = [pltpu.make_async_copy(src, dst, loc_sem.at[k]) for k, (src, dst) in enumerate(pairs)]
     for copy in local:
         copy.start()
-    for copy in local:
-        copy.wait()
-    turned = [TW[k].T for k in range(2)]
-    for k in range(2):
-        for t in range(5):
-            at = pl.multiple_of(c * 1536 + t * 256 + k * LANES, LANES)
-            GU[zl, y, :, pl.ds(at, LANES)] = turned[k][:, t * LANES:(t + 1) * LANES]
-    ends = [w[:, MAIN:W] for w in turned]
-    both = jnp.concatenate([ends[0], ends[1]], axis=1).astype(jnp.float32)
-    swapped = jnp.concatenate([ends[1], ends[0]], axis=1).astype(jnp.float32)
-    pick = jnp.where(c == 0, both, swapped)
-    GU[zl, y, :, pl.ds(pl.multiple_of(1280 + c * LANES, LANES), LANES)] = pick.astype(jnp.bfloat16)
-    for ref, base in ((TG, 0), (TU, 3)):
-        v = ref[...]
-        TAPS[base:base + 3, 0:MAIN] = v[:, 0:MAIN]
-        TAPS[base:base + 3, MAIN:WP] = jnp.concatenate([v[:, MAIN:W], v[:, W + MAIN:GW]], axis=1)
-        TAPS[base:base + 3, WP:GW] = v[:, W:W + MAIN]
+    for k in (2, 3):
+        local[k].wait()
+
+    def build():
+        for k in (0, 1, 4, 5, 6, 7, 8, 9, 10, 11):
+            local[k].wait()
+        turned = [TW[k].T for k in range(2)]
+        for k in range(2):
+            for t in range(5):
+                at = pl.multiple_of(c * 1536 + t * 256 + k * LANES, LANES)
+                GU[zl, y, :, pl.ds(at, LANES)] = turned[k][:, t * LANES:(t + 1) * LANES]
+        ends = [w[:, MAIN:W] for w in turned]
+        both = jnp.concatenate([ends[0], ends[1]], axis=1).astype(jnp.float32)
+        swapped = jnp.concatenate([ends[1], ends[0]], axis=1).astype(jnp.float32)
+        pick = jnp.where(c == 0, both, swapped)
+        GU[zl, y, :, pl.ds(pl.multiple_of(1280 + c * LANES, LANES), LANES)] = pick.astype(jnp.bfloat16)
+        for ref, base in ((TG, 0), (TU, 3)):
+            v = ref[...]
+            TAPS[base:base + 3, 0:MAIN] = v[:, 0:MAIN]
+            TAPS[base:base + 3, MAIN:WP] = jnp.concatenate([v[:, MAIN:W], v[:, W + MAIN:GW]], axis=1)
+            TAPS[base:base + 3, WP:GW] = v[:, W:W + MAIN]
+
     with jax.named_scope("barrier_wait"):
         pl.semaphore_wait(barrier, len(greeted))
 
-    yz = (y_up, y_down, z_up, z_down, y_far, z_far)
-    zy = (z_up, z_down, y_up, y_down, z_far, y_far)
+    yz = (y_up, y_down, z_up, z_down)
+    zy = (z_up, z_down, y_up, y_down)
 
     def region(ref, rows, cols=None):
         def at(i, j, sub=None):
@@ -269,10 +246,10 @@
         )
 
     pool = pair(
-        Direct,
+        Relay,
         region(POOL.at[2 * c], (0, 32)), region(POOL.at[2 * c + 1], (0, 32)),
         region(POOL.at[2 * (1 - c)], (0, 32)), region(POOL.at[2 * (1 - c) + 1], (0, 32)),
-        0,
+        0, split=0,
     )
     gu = pair(
         Relay,
@@ -345,7 +322,7 @@
 
             lax.fori_loop(0, 4, strip, 0)
 
-    def post(b, keep):
+    def post(b, n, keep):
         for g in range(4):
             cols = slice(g * 512, (g + 1) * 512)
             MIX[:, cols] = jnp.dot(
@@ -380,7 +357,7 @@
             scale = SC[rows16(i), :]
             for t in range(D // LANES):
                 cols = slice(t * LANES, (t + 1) * LANES)
-                X[b, rows16(i), cols] = (keep[rows16(i), cols] * scale * GAINS[2, :, cols]).astype(jnp.bfloat16)
+                X[n, rows16(i), cols] = (keep[rows16(i), cols] * scale * GAINS[2, :, cols]).astype(jnp.bfloat16)
             return 0
 
         lax.fori_loop(0, OUTR // 16, scaled, 0)
@@ -388,10 +365,14 @@
     def start_of(b):
         return (2 * b + c) * ROWS
 
-    def hidden(b, begin, stop):
+    def hidden(n, count, begin, stop):
+        size = count * OUTR
+        left = X[n] if count == 1 else X[n:n + count].reshape(size, D)
+
         def project(i, ref):
             w = GU[:, :, :, pl.ds(pl.multiple_of(i * 256, 256), 256)].reshape(D, 256)
-            ref[...] = jnp.dot(X[b], w, preferred_element_type=jnp.float32).astype(jnp.bfloat16).astype(jnp.float32)
+            pre = jnp.dot(left, w, preferred_element_type=jnp.float32).astype(jnp.bfloat16).astype(jnp.float32)
+            ref[0:size, :] = pre
 
         def conv(v, taps_at, base):
             taps = TAPS[base:base + 3, pl.ds(taps_at, LANES)]
@@ -399,15 +380,17 @@
 
         def act(ref, i, ends):
             at = i * LANES if ends else pl.multiple_of(i * LANES, LANES)
-            for row in (0, 96):
-                gate, up = ref[row:row + 112, 0:LANES], ref[row:row + 112, LANES:]
-                if ends:
-                    lead = lax.broadcasted_iota(jnp.int32, (112, LANES), 1) < 64
-                    gate, up = jnp.where(lead, gate, up), pltpu.roll(jnp.where(lead, up, gate), 64, 1)
-                gate, up = conv(gate, at, 0)[16:], conv(up, at, 3)[16:]
-                inner = 0.7978845608028654 * (gate + 0.044715 * gate * gate * gate)
-                value = 0.5 * gate * (1.0 + jnp.tanh(inner)) * up
-                HID[b, row:row + 96, pl.ds(at, LANES)] = value.astype(jnp.bfloat16)
+            for k in range(count):
+                for row in (0, 96):
+                    here = slice(k * OUTR + row, k * OUTR + row + 112)
+                    gate, up = ref[here, 0:LANES], ref[here, LANES:]
+                    if ends:
+                        lead = lax.broadcasted_iota(jnp.int32, (112, LANES), 1) < 64
+                        gate, up = jnp.where(lead, gate, up), pltpu.roll(jnp.where(lead, up, gate), 64, 1)
+                    gate, up = conv(gate, at, 0)[16:], conv(up, at, 3)[16:]
+                    inner = 0.7978845608028654 * (gate + 0.044715 * gate * gate * gate)
+                    value = 0.5 * gate * (1.0 + jnp.tanh(inner)) * up
+                    HID[n + k, row:row + 96, pl.ds(at, LANES)] = value.astype(jnp.bfloat16)
 
         def order(i):
             return i + jnp.minimum(lax.div(i, 5), 1) - 6 * lax.div(i, 10)
@@ -449,44 +432,61 @@
     first, second = pl.ds(0, 96), pl.ds(96, 96)
     push(XB.at[x, last], XB.at[ring(x + c, 4), top], 4, after)
     for g in pool:
-        g.start()
-    for g in gu:
         g.start_p()
+    for g in pool:
+        g.start_s()
     push(XB.at[x, body], XB.at[x, body], 0, x_up)
     push(XB.at[x, body], XB.at[x, body], 1, x_down)
-    for g in pool:
-        g.p()
-    for g in gu:
-        g.start_s()
-    for g in gu:
+    build()
+    for g in gu:
+        g.start_p()
+    for g in pool:
         g.p1f()
-    for g in gu:
+    for g in pool:
         g.p1s()
     arrived(XB.at[x, top], 4)
     prep(x, start_of(x))
     for g in pool:
-        g.r()
-    for g in pool:
-        g.join()
-    post(x, AM)
-    for g in gu:
         g.p2()
-    for g in gu:
+    for g in pool:
         g.q0()
+    for g in pool:
+        g.q1()
+    for g in pool:
+        g.q2()
+    for g in gu:
+        g.start_s()
+    for g in gu:
+        g.p1f()
+    for g in pool:
+        g.q3()
+    for g in gu:
+        g.p1s()
+    for g in pool:
+        g.r012()
+    for g in pool:
+        g.r3()
     arrived(XB.at[low, body], 0)
     push(XB.at[low, head], XB.at[low, head], 2, x_up)
     arrived(XB.at[high, body], 1)
     push(XB.at[high, tail], XB.at[high, tail], 3, x_down)
     side(0, high)
+    for g in pool:
+        g.join()
+    post(x, 3, AM)
+    for g in gu:
+        g.p2()
+    for g in gu:
+        g.q0()
     arrived(XB.at[high, top], 5)
     prep(high, start_of(high))
-    post(high, AF)
+    post(high, 1, AF)
     for g in gu:
         g.q1()
+    for g in dn:
+        g.start_p()
     for g in gu:
         g.q2()
-    for g in dn:
-        g.start_p()
     arrived(XB.at[far, head], 2)
     arrived(XB.at[far, tail], 3)
     side(1, far)
@@ -497,75 +497,81 @@
     for g in dn:
         g.start_s()
     prep(far, start_of(far))
-    post(far, AF)
-    for g in dn:
-        g.p1f()
-    for g in dn:
-        g.p1s()
-    for g in gu:
-        g.r()
+    post(far, 0, AF)
     arrived(XB.at[low, top], 7)
     prep(low, start_of(low))
     for g in dn:
+        g.p1f()
+    for g in dn:
+        g.p1s()
+    post(low, 2, AF)
+    for g in gu:
+        g.r012()
+    for g in gu:
+        g.r3()
+    for g in gu:
+        g.join()
+    hidden(0, 1, 0, 1)
+    for g in dn:
         g.p2()
-    post(low, AF)
+    hidden(0, 1, 1, 3)
     for g in dn:
         g.q0()
-    for g in gu:
-        g.join()
-    hidden(far, 0, 3)
     for g in dn:
         g.q1()
+    hidden(0, 1, 3, 5)
     for g in dn:
         g.q2()
-    hidden(far, 3, 5)
+    hidden(1, 2, 0, 1)
     for g in dn:
         g.q3()
-    hidden(high, 0, 3)
+    hidden(1, 2, 1, 2)
+    for g in dn:
+        g.r012()
     for g in dn:
         g.join1()
-    down(far, 0)
-    push(SB.at[far, pl.ds(0, 8), first], RB.at[0, pl.ds(0, 8)], 8, x_up)
-    push(SB.at[far, pl.ds(0, 8), second], RB.at[1, pl.ds(0, 8)], 9, x_down)
-    for g in dn:
-        g.r()
-    hidden(high, 3, 5)
+    down(0, 0)
+    push(SB.at[0, pl.ds(0, 8), first], RB.at[0, pl.ds(0, 8)], 8, x_up)
+    push(SB.at[0, pl.ds(0, 8), second], RB.at[1, pl.ds(0, 8)], 9, x_down)
+    hidden(1, 2, 2, 3)
+    for g in dn:
+        g.r3()
     for g in dn:
         g.join2()
-    down(far, 1)
-    push(SB.at[far, pl.ds(8, 8), first], RB.at[0, pl.ds(8, 8)], 14, x_up)
-    push(SB.at[far, pl.ds(8, 8), second], RB.at[1, pl.ds(8, 8)], 15, x_down)
-    down(high, 0)
-    push(SB.at[high, pl.ds(0, 8), second], R.at[0, pl.ds(0, 8), second], 10, x_up)
-    hidden(low, 0, 5)
-    down(low, 0)
-    push(SB.at[low, pl.ds(0, 8), first], R.at[1, pl.ds(0, 8), first], 11, x_down)
-    down(high, 1)
-    push(SB.at[high, pl.ds(8, 8), second], R.at[0, pl.ds(8, 8), second], 16, x_up)
-    down(low, 1)
-    push(SB.at[low, pl.ds(8, 8), first], R.at[1, pl.ds(8, 8), first], 17, x_down)
+    down(0, 1)
+    push(SB.at[0, pl.ds(8, 8), first], RB.at[0, pl.ds(8, 8)], 14, x_up)
+    push(SB.at[0, pl.ds(8, 8), second], RB.at[1, pl.ds(8, 8)], 15, x_down)
+    hidden(1, 2, 3, 5)
+    down(1, 0)
+    push(SB.at[1, pl.ds(0, 8), second], R.at[0, pl.ds(0, 8), second], 10, x_up)
+    down(2, 0)
+    push(SB.at[2, pl.ds(0, 8), first], R.at[1, pl.ds(0, 8), first], 11, x_down)
+    down(1, 1)
+    push(SB.at[1, pl.ds(8, 8), second], R.at[0, pl.ds(8, 8), second], 16, x_up)
+    down(2, 1)
+    push(SB.at[2, pl.ds(8, 8), first], R.at[1, pl.ds(8, 8), first], 17, x_down)
     arrived(RB.at[0, pl.ds(0, 8)], 8)
-    relay(high, 0, 0, 0)
-    push(SB.at[high, pl.ds(0, 8), first], R.at[0, pl.ds(0, 8), first], 12, x_up)
+    relay(1, 0, 0, 0)
+    push(SB.at[1, pl.ds(0, 8), first], R.at[0, pl.ds(0, 8), first], 12, x_up)
     arrived(RB.at[1, pl.ds(0, 8)], 9)
-    relay(low, 96, 1, 0)
-    push(SB.at[low, pl.ds(0, 8), second], R.at[1, pl.ds(0, 8), second], 13, x_down)
+    relay(2, 96, 1, 0)
+    push(SB.at[2, pl.ds(0, 8), second], R.at[1, pl.ds(0, 8), second], 13, x_down)
     arrived(RB.at[0, pl.ds(8, 8)], 14)
-    relay(high, 0, 0, 1)
-    push(SB.at[high, pl.ds(8, 8), first], R.at[0, pl.ds(8, 8), first], 18, x_up)
+    relay(1, 0, 0, 1)
+    push(SB.at[1, pl.ds(8, 8), first], R.at[0, pl.ds(8, 8), first], 18, x_up)
     arrived(RB.at[1, pl.ds(8, 8)], 15)
-    relay(low, 96, 1, 1)
-    push(SB.at[low, pl.ds(8, 8), second], R.at[1, pl.ds(8, 8), second], 19, x_down)
-    hidden(x, 0, 5)
-    down(x, 0)
-    down(x, 1)
+    relay(2, 96, 1, 1)
+    push(SB.at[2, pl.ds(8, 8), second], R.at[1, pl.ds(8, 8), second], 19, x_down)
+    hidden(3, 1, 0, 5)
+    down(3, 0)
+    down(3, 1)
 
     def last_rows(i, _):
         r = rows16(i)
         total = jnp.zeros((16, LANES), jnp.float32)
         values = []
         for k in range(16):
-            v = SB[x, k, r].astype(jnp.float32) + R[0, k, r].astype(jnp.float32) + R[1, k, r].astype(jnp.float32)
+            v = SB[3, k, r].astype(jnp.float32) + R[0, k, r].astype(jnp.float32) + R[1, k, r].astype(jnp.float32)
             values.append(v)
             total = total + v * v
         scale = lax.rsqrt(jnp.sum(total, axis=-1, keepdims=True) * (1.0 / D) + eps)
@@ -625,8 +631,8 @@
             pltpu.VMEM((4, 4, 128, 2 * GW), bf16),
             pltpu.VMEM((4, 4, GW, LANES), bf16),
             pltpu.VMEM((4, OUTR, D), bf16),
-            pltpu.VMEM((OUTR, 256), f32),
-            pltpu.VMEM((OUTR, 256), f32),
+            pltpu.VMEM((2 * OUTR, 256), f32),
+            pltpu.VMEM((2 * OUTR, 256), f32),
             pltpu.VMEM((4, ROWS, GW), bf16),
             pltpu.VMEM((4, 16, ROWS, LANES), bf16),
             pltpu.VMEM((2, 16, 96, LANES), bf16),
@@ -639,7 +645,7 @@
             pltpu.VMEM((4, 1, D), f32),
             pltpu.SemaphoreType.DMA((12,)),
             pltpu.SemaphoreType.DMA((6, 5)),
-            pltpu.SemaphoreType.DMA((6, 16)),
+            pltpu.SemaphoreType.DMA((6, 19)),
             pltpu.SemaphoreType.DMA((3,)),
             pltpu.SemaphoreType.DMA((20,)),
         ],

time: 98 us -> 96.2 us (0.982)
  Pallas kernels: 95.7 us -> 94 us
    pallas_call x1, Pallas kernels: 95.7 us -> 94 us  [shards(): pl.pallas_call(layer, out_shape=jax.ShapeDtypeStruct((ROWS, D), bf16), in...]
where the time goes in v3:
time: 96.2 us; the launch traced here: 96.1 us
  Pallas kernels  94 us (98%)
  local copies, waits for them, and re-layouts  2.09 us (2%)
    pallas_call x1, Pallas kernels, shards(): pl.pallas_call(layer, out_shape=jax.ShapeDtypeStruct((ROWS, D), bf16), in...  94 us
    unnamed x1, local copies, waits for them, and re-layouts  2.09 us

profile of v3, /device:TPU:1, one launch (start us, length us, event | category | flops | bytes accessed | tf_op | source)
XLA Modules:
  0.0 96.1 jit_solution(9233036995906409113)
XLA Ops:
  0.0 94.0 %shard_map.109 = bf16[192,2048]{1,0:T(8,128)(2,1)} custom-call(bf16[192,2048]{1,0:T(8,128)(2,1)} %tokens.1, bf16[4,32,512]{2,1,0:T(8,128)(2,1)} %pool_w.1, bf16[704,128]{1,0:T(8,128)(2,1)} %bitcast.6, bf16[704,128]{1,0:T(8,128)(2,1)} %bitcast.7, bf16[704,128]{1,0:T(8,128)(2,1)} %dn_w.1, f32[3,5632]{1,0:T(4,128)} %gate_taps.1, f32[3,5632]{1,0:T(4,128)} %up_taps.1, ...), custom_call_target="tpu_custom_call" | custom-call | tf_op jit(solution)/shard_map/pallas_call | solution.py:619
  94.0 2.1 %copy.13 = bf16[192,2048]{1,0:T(8,128)(2,1)} copy(bf16[192,2048]{1,0:T(8,128)(2,1)} %shard_map.109) | data formatting | bytes 1572864

commit v4 on v3

--- a/solution.py
+++ b/solution.py
@@ -566,30 +566,42 @@
     down(3, 0)
     down(3, 1)
 
+    def summed(k, r):
+        return SB[3, k, r].astype(jnp.float32) + R[0, k, r].astype(jnp.float32) + R[1, k, r].astype(jnp.float32)
+
+    def first_rows(i, _):
+        r = rows16(i)
+        total = jnp.zeros((16, LANES), jnp.float32)
+        for k in range(8):
+            v = summed(k, r)
+            AF[r, k * LANES:(k + 1) * LANES] = v
+            total = total + v * v
+        SC[r, :] = total
+        return 0
+
     def last_rows(i, _):
         r = rows16(i)
-        total = jnp.zeros((16, LANES), jnp.float32)
+        total = SC[r, :]
         values = []
-        for k in range(16):
-            v = SB[3, k, r].astype(jnp.float32) + R[0, k, r].astype(jnp.float32) + R[1, k, r].astype(jnp.float32)
+        for k in range(8, 16):
+            v = summed(k, r)
             values.append(v)
             total = total + v * v
         scale = lax.rsqrt(jnp.sum(total, axis=-1, keepdims=True) * (1.0 / D) + eps)
         for k in range(16):
             cols = pl.ds(pl.multiple_of((slots[k][0] * 4 + slots[k][1]) * LANES, LANES), LANES)
             a = AM[pl.ds(pl.multiple_of(i * 16 + 16, 16), 16), cols]
-            out[r, cols] = (a + values[k] * scale * GAINS[3, :, cols]).astype(jnp.bfloat16)
+            v = AF[r, k * LANES:(k + 1) * LANES] if k < 8 else values[k - 8]
+            out[r, cols] = (a + v * scale * GAINS[3, :, cols]).astype(jnp.bfloat16)
         return 0
 
-    arrived(R.at[0, pl.ds(0, 8), second], 10)
-    arrived(R.at[1, pl.ds(0, 8), first], 11)
-    arrived(R.at[0, pl.ds(0, 8), first], 12)
-    arrived(R.at[1, pl.ds(0, 8), second], 13)
-    arrived(R.at[0, pl.ds(8, 8), second], 16)
-    arrived(R.at[1, pl.ds(8, 8), first], 17)
-    arrived(R.at[0, pl.ds(8, 8), first], 18)
-    arrived(R.at[1, pl.ds(8, 8), second], 19)
-    lax.fori_loop(0, ROWS // 16, last_rows, 0, unroll=2)
+    for p in range(2):
+        here = pl.ds(8 * p, 8)
+        arrived(R.at[0, here, second], 10 + 6 * p)
+        arrived(R.at[1, here, first], 11 + 6 * p)
+        arrived(R.at[0, here, first], 12 + 6 * p)
+        arrived(R.at[1, here, second], 13 + 6 * p)
+        lax.fori_loop(0, ROWS // 16, last_rows if p else first_rows, 0, unroll=2)
     with jax.named_scope("drain"):
         pushed(XB.at[pl.ds(0, 3), pl.ds(0, ROWS)], 0)
         pushed(XB.at[0, pl.ds(0, 4 * HALO)], 1)

time: 96.2 us -> 96 us (level)
  no operation moved by 1% of the time
where the time goes in v4:
time: 96 us; the launch traced here: 95.9 us
  Pallas kernels  93.8 us (98%)
  local copies, waits for them, and re-layouts  2.09 us (2%)
    pallas_call x1, Pallas kernels, shards(): pl.pallas_call(layer, out_shape=jax.ShapeDtypeStruct((ROWS, D), bf16), in...  93.8 us
    unnamed x1, local copies, waits for them, and re-layouts  2.09 us

profile of v4, /device:TPU:1, one launch (start us, length us, event | category | flops | bytes accessed | tf_op | source)
XLA Modules:
  0.0 95.9 jit_solution(5252071945343158191)
XLA Ops:
  0.0 93.8 %shard_map.109 = bf16[192,2048]{1,0:T(8,128)(2,1)} custom-call(bf16[192,2048]{1,0:T(8,128)(2,1)} %tokens.1, bf16[4,32,512]{2,1,0:T(8,128)(2,1)} %pool_w.1, bf16[704,128]{1,0:T(8,128)(2,1)} %bitcast.6, bf16[704,128]{1,0:T(8,128)(2,1)} %bitcast.7, bf16[704,128]{1,0:T(8,128)(2,1)} %dn_w.1, f32[3,5632]{1,0:T(4,128)} %gate_taps.1, f32[3,5632]{1,0:T(4,128)} %up_taps.1, ...), custom_call_target="tpu_custom_call" | custom-call | tf_op jit(solution)/shard_map/pallas_call | solution.py:631
  93.8 2.1 %copy.13 = bf16[192,2048]{1,0:T(8,128)(2,1)} copy(bf16[192,2048]{1,0:T(8,128)(2,1)} %shard_map.109) | data formatting | bytes 1572864
